TPU v7x, 256 devices: a whole 4x4x8 slice. The times are simulated.
256 devices in a mesh: sp: 64 (over z, x, core), tp: 4 (over y).
Axes of the slice: x: 4, y: 4, z: 8, core: 2. Of those that a mesh axis runs over, the one named last changes fastest.
Arguments:
- residual: bfloat16 [16384, 2048], P('sp', 'tp'), may hold values from -48 to 48
- queries: bfloat16 [16384, 1024], P('sp', 'tp'), may hold values from -6 to 6
- key_rows: bfloat16 [16384, 512], P('sp', 'tp'), may hold values from -6 to 6
- value_rows: bfloat16 [16384, 512], P('sp', 'tp'), may hold values from -6 to 6
- break_shift: bfloat16 [4, 16384], P('tp', 'sp'), may hold values from -20 to 0
- head_gain: float32 [1024], P('tp'), may hold values from 0.1 to 1.9
- out_weight: bfloat16 [1024, 2048], P('tp'), may hold values from -0.1875 to 0.1875
- mlp_gain: float32 [2048], replicated, may hold values from 0.1 to 1.9
- up_weight: bfloat16 [2048, 8192], P('sp', 'tp'), may hold values from -0.125 to 0.125
- down_weight: bfloat16 [8192, 2048], P('tp', 'sp'), may hold values from -0.0625 to 0.0625
Outputs:
- layer_out: bfloat16 [16384, 2048], P('sp', 'tp')
All inputs are finite; a program needn't handle non-finite values.
Results may differ from a plain program's by a relative error of at most 0.013.
Values may be sent and summed in bfloat16 or wider, within the bound.
A program may use at most 128 MiB of HBM per device.

v0:
```python
import jax
import jax.numpy as jnp
from jax import lax
from jax.sharding import PartitionSpec as P

HEAD_DIM = 128


eps = 1e-06


def turned_gather(arrays, axis, dims):
    turned = [jnp.moveaxis(a, dim, 0) for a, dim in zip(arrays, dims)]
    widths = [t[0].size for t in turned]
    both = jnp.concatenate([t.reshape(-1, w) for t, w in zip(turned, widths)], axis=1)
    result = lax.all_gather(both, axis, axis=0, tiled=True)
    pieces = jnp.split(result, [sum(widths[:k]) for k in range(1, len(widths))], axis=1)
    return tuple(
        (
            jnp.moveaxis(b.reshape(-1, *t.shape[1:]), 0, dim)
            for b, t, dim in zip(pieces, turned, dims)
        )
    )


def in_blocks(array, dim, size):
    dims = array.shape
    pieces = array.reshape(*dims[:dim], size, dims[dim] // size, *dims[dim + 1 :])
    return jnp.moveaxis(pieces, dim, 0)


def sent_and_summed(array, axis, dim):
    size = lax.axis_size(axis)
    pieces = lax.all_to_all(in_blocks(array, dim, size), axis, 0, 0, tiled=True)
    return jnp.sum(pieces.astype(jnp.float32), axis=0)


def sent_to_all(array, axis):
    size = lax.axis_size(axis)
    return lax.all_to_all(
        jnp.broadcast_to(array[None], (size, *array.shape)), axis, 0, 0, tiled=True
    )


def of_everyone(array, axis):
    return sent_to_all(array, axis).sum(axis=0)


def joined_along(pieces, dim):
    dims = list(pieces.shape[1:])
    dims[dim] *= pieces.shape[0]
    return jnp.moveaxis(pieces, 0, dim).reshape(dims)


def collect(array, axis, dim):
    return joined_along(sent_to_all(array, axis), dim)


def stick_attention(queries, key_all, value_all, shift_all, first_pos, key_block):
    token_count = queries.shape[0]
    kv_local = key_all.shape[1] // HEAD_DIM
    query_local = queries.shape[1] // HEAD_DIM
    group_size = query_local // kv_local
    stacked = queries.reshape(token_count, kv_local, group_size, HEAD_DIM).transpose(1, 2, 0, 3)
    stacked = stacked.reshape(kv_local, group_size * token_count, HEAD_DIM)
    query_pos = first_pos + lax.iota(jnp.int32, group_size * token_count) % token_count
    score_scale = HEAD_DIM ** (-0.5)
    block_count = (first_pos + token_count - 1 + key_block - 1) // key_block

    def one_block(turn_index, state_pair):
        running, broken_after = state_pair
        offset = (block_count - 1 - turn_index) * key_block
        key_block_rows = lax.dynamic_slice_in_dim(key_all, offset, key_block, 0).reshape(
            key_block, kv_local, HEAD_DIM
        )
        value_block_rows = lax.dynamic_slice_in_dim(value_all, offset, key_block, 0).reshape(
            key_block, kv_local, HEAD_DIM
        )
        shift_block = lax.dynamic_slice_in_dim(shift_all, offset, key_block, 1).astype(jnp.float32)
        scores = jnp.einsum(
            "grd,kgd->grk", stacked, key_block_rows, preferred_element_type=jnp.float32
        )
        scores = scores * score_scale + shift_block[:, None, :]
        key_pos = offset + lax.iota(jnp.int32, key_block)
        visible = key_pos[None, None, :] < query_pos[None, :, None]
        broken = jnp.where(visible, jax.nn.log_sigmoid(-scores), 0.0)
        later = lax.cumsum(broken, axis=2, reverse=True) - broken + broken_after[:, :, None]
        weights = jnp.where(visible, jnp.exp(jax.nn.log_sigmoid(scores) + later), 0.0).astype(
            jnp.bfloat16
        )
        running = running + jnp.einsum(
            "grk,kgd->grd", weights, value_block_rows, preferred_element_type=jnp.float32
        )
        return (running, broken_after + jnp.sum(broken, axis=2))

    start_pair = (
        jnp.zeros((kv_local, group_size * token_count, HEAD_DIM), jnp.float32),
        jnp.zeros((kv_local, group_size * token_count), jnp.float32),
    )
    running, broken_after = lax.fori_loop(0, block_count, one_block, start_pair)
    running = running.reshape(kv_local, group_size, token_count, HEAD_DIM).transpose(2, 0, 1, 3)
    return running.reshape(token_count, query_local, HEAD_DIM)


def body(
    residual,
    queries,
    key_rows,
    value_rows,
    break_shift,
    head_gain,
    out_weight,
    mlp_gain,
    up_weight,
    down_weight,
):
    token_count = queries.shape[0]
    first_pos = lax.axis_index("sp") * token_count
    up_whole, down_whole = turned_gather((up_weight, down_weight), "sp", (0, 1))
    key_all, value_all, shift_all = turned_gather(
        (key_rows, value_rows, break_shift), "sp", (0, 0, 1)
    )
    key_block = min(2048, key_all.shape[0])
    mixed = stick_attention(queries, key_all, value_all, shift_all, first_pos, key_block)
    power = jnp.mean(mixed * mixed, axis=2, keepdims=True)
    attended = (mixed * lax.rsqrt(power + eps) * head_gain.reshape(-1, HEAD_DIM)).astype(
        jnp.bfloat16
    )
    attended = attended.reshape(token_count, -1)
    partial_value = jnp.dot(attended, out_weight, preferred_element_type=jnp.float32)
    column_count = residual.shape[1]
    column_start = lax.axis_index("tp") * column_count
    summed = sent_and_summed(partial_value.astype(jnp.bfloat16), "tp", 1)
    hidden_state = (residual.astype(jnp.float32) + summed).astype(jnp.bfloat16)
    widened = hidden_state.astype(jnp.float32)
    squares = of_everyone(jnp.sum(widened * widened, axis=1), "tp")
    gain_slice = lax.dynamic_slice_in_dim(mlp_gain, column_start, column_count, 0)
    inverse = lax.rsqrt(squares[:, None] / mlp_gain.shape[0] + eps)
    normed = (widened * inverse * gain_slice).astype(jnp.bfloat16)
    mlp_in = collect(normed, "tp", 1)
    lifted = jnp.dot(mlp_in, up_whole, preferred_element_type=jnp.float32)
    activated = jnp.square(jax.nn.relu(lifted)).astype(jnp.bfloat16)
    expanded = jnp.dot(activated, down_whole, preferred_element_type=jnp.float32)
    mlp_total = sent_and_summed(expanded.astype(jnp.bfloat16), "tp", 1)
    return (hidden_state.astype(jnp.float32) + mlp_total).astype(jnp.bfloat16)


def solution(mesh):
    in_specs = (
        P("sp", "tp"),
        P("sp", "tp"),
        P("sp", "tp"),
        P("sp", "tp"),
        P("tp", "sp"),
        P("tp"),
        P("tp", None),
        P(),
        P("sp", "tp"),
        P("tp", "sp"),
    )
    out_specs = P("sp", "tp")
    return jax.shard_map(body, mesh=mesh, in_specs=in_specs, out_specs=out_specs, check_vma=False)
```

profile of v0, /device:TPU:224, one launch (start us, length us, event | category | flops | bytes accessed | tf_op | source)
XLA Modules:
  0.0 419.3 jit_solution(12546519314148546603)
XLA Ops:
  11.8 86.7 %all-gather.3.cloned.1.call-done = bf16[16384,257]{1,0:T(8,128)(2,1)} async-done(((bf16[256,257]{1,0:T(8,128)(2,1)}), bf16[16384,257]{1,0:T(8,128)(2,1)}) %all-gather.3.cloned.1.call-update) | async-done | bytes 8421392 | tf_op jit(solution)/shard_map/all_gather | solution.py:16
  98.5 2.9 slice_reduce_fusion
  101.4 5.9 %fusion.53 = (bf16[16384,128]{1,0:T(8,128)(2,1)}, bf16[16384,128]{1,0:T(8,128)(2,1)}) fusion(bf16[16384,257]{1,0:T(8,128)(2,1)} %all-gather.3.cloned.1.call-done), kind=kLoop, calls=%fused_computation.74 | loop fusion | bytes 16777216 | tf_op jit(solution)/shard_map/split | solution.py:17
  107.4 232.4 %while.15 = (s32[]{:T(128)}, f32[1,512,128]{2,1,0:T(8,128)S(1)}, f32[1,512]{1,0:T(1,128)S(1)}, s32[]{:T(128)}, s32[]{:T(128)}, /*index=5*/bf16[16384,128]{1,0:T(...) while((s32[]{:T(128)}, f32[1,512,128]{2,1,0:T(8,128)S(1)}, ...), condition=%wide.region_4.5_spmd.clone, body=%wide.region_0.4_spmd.clone.sunk | while | flops 700652544 | bytes 60725496 | solution.py:100
  107.4 5.5 %fusion.70 = (f32[512]{0:T(512)S(1)}, f32[512,2048]{0,1:T(8,128)S(1)}, f32[2048,512]{1,0:T(8,128)}) fusion(f32[2048]{0:T(1024)S(1)} %bitcast.116, s32[512]{0:T(512)S(1)} %fusion.69, s32[2048]{0:T(1024)S(1)} %iota_add_fusion.2, bf16[1,512,128]{2,1,0:T(8,128)(2,1)S(1)} %get-tuple-element.274, bf16[16384,128]{1,0:T(8,128)(2,1)} %get-tuple-element.273, ...), kind=kOutput, calls=%fused_computation.73.clone.1 | convolution fusion | flops 281017856 | bytes 9064452 | tf_op jit(solution)/shard_map/while/body/grd,kgd->grk/dot_general | solution.py:80
  113.0 10.1 %fusion.71 = f32[1,512,16,128]{1,2,3,0:T(8,128)S(1)} fusion(f32[1,512,16,128]{1,3,2,0:T(8,128)S(1)} %bitcast.108), kind=kOutput, calls=%fused_computation.20.clone.1 | output fusion | flops 133169152 | bytes 8388608 | tf_op jit(solution)/shard_map/reduce-window.4
  123.0 4.4 %copy.62 = f32[1,512,16,128]{1,3,2,0:T(8,128)} copy(f32[1,512,16,128]{1,2,3,0:T(8,128)S(1)} %fusion.71) | data formatting | bytes 8388608 | tf_op jit(solution)/shard_map/reduce-window.4
  127.6 7.0 %fusion.72 = bf16[512,2048]{0,1:T(8,128)(2,1)S(1)} fusion(f32[512,2048]{0,1:T(8,128)} %copy-done.1, f32[1,512,16,128]{1,3,2,0:T(8,128)} %copy.62, f32[2048,512]{1,0:T(8,128)} %get-tuple-element.236, f32[512]{0:T(512)S(1)} %bitcast.118, f32[512,16]{0,1:T(8,128)S(1)} %slice_bitcast_fusion.5, f32[2048]{0:T(1024)S(1)} %bitcast.117, s32[512]{0:T(512)S(1)} %fusion.69, ...), kind=kLoop, calls=%fused_computation.5.clone.1 | loop fusion | flops 17825792 | bytes 14733312 | tf_op jit(solution)/shard_map/while/body/convert_element_type | solution.py:88
  134.5 1.8 fusion.73
  136.4 5.5 %fusion.70 = (f32[512]{0:T(512)S(1)}, f32[512,2048]{0,1:T(8,128)S(1)}, f32[2048,512]{1,0:T(8,128)}) fusion(f32[2048]{0:T(1024)S(1)} %bitcast.116, s32[512]{0:T(512)S(1)} %fusion.69, s32[2048]{0:T(1024)S(1)} %iota_add_fusion.2, bf16[1,512,128]{2,1,0:T(8,128)(2,1)S(1)} %get-tuple-element.274, bf16[16384,128]{1,0:T(8,128)(2,1)} %get-tuple-element.273, ...), kind=kOutput, calls=%fused_computation.73.clone.1 | convolution fusion | flops 281017856 | bytes 9064452 | tf_op jit(solution)/shard_map/while/body/grd,kgd->grk/dot_general | solution.py:80
  142.0 10.1 %fusion.71 = f32[1,512,16,128]{1,2,3,0:T(8,128)S(1)} fusion(f32[1,512,16,128]{1,3,2,0:T(8,128)S(1)} %bitcast.108), kind=kOutput, calls=%fused_computation.20.clone.1 | output fusion | flops 133169152 | bytes 8388608 | tf_op jit(solution)/shard_map/reduce-window.4
  152.1 4.4 %copy.62 = f32[1,512,16,128]{1,3,2,0:T(8,128)} copy(f32[1,512,16,128]{1,2,3,0:T(8,128)S(1)} %fusion.71) | data formatting | bytes 8388608 | tf_op jit(solution)/shard_map/reduce-window.4
  156.6 7.2 %fusion.72 = bf16[512,2048]{0,1:T(8,128)(2,1)S(1)} fusion(f32[512,2048]{0,1:T(8,128)} %copy-done.1, f32[1,512,16,128]{1,3,2,0:T(8,128)} %copy.62, f32[2048,512]{1,0:T(8,128)} %get-tuple-element.236, f32[512]{0:T(512)S(1)} %bitcast.118, f32[512,16]{0,1:T(8,128)S(1)} %slice_bitcast_fusion.5, f32[2048]{0:T(1024)S(1)} %bitcast.117, s32[512]{0:T(512)S(1)} %fusion.69, ...), kind=kLoop, calls=%fused_computation.5.clone.1 | loop fusion | flops 17825792 | bytes 14733312 | tf_op jit(solution)/shard_map/while/body/convert_element_type | solution.py:88
  165.7 5.5 %fusion.70 = (f32[512]{0:T(512)S(1)}, f32[512,2048]{0,1:T(8,128)S(1)}, f32[2048,512]{1,0:T(8,128)}) fusion(f32[2048]{0:T(1024)S(1)} %bitcast.116, s32[512]{0:T(512)S(1)} %fusion.69, s32[2048]{0:T(1024)S(1)} %iota_add_fusion.2, bf16[1,512,128]{2,1,0:T(8,128)(2,1)S(1)} %get-tuple-element.274, bf16[16384,128]{1,0:T(8,128)(2,1)} %get-tuple-element.273, ...), kind=kOutput, calls=%fused_computation.73.clone.1 | convolution fusion | flops 281017856 | bytes 9064452 | tf_op jit(solution)/shard_map/while/body/grd,kgd->grk/dot_general | solution.py:80
  171.2 10.1 %fusion.71 = f32[1,512,16,128]{1,2,3,0:T(8,128)S(1)} fusion(f32[1,512,16,128]{1,3,2,0:T(8,128)S(1)} %bitcast.108), kind=kOutput, calls=%fused_computation.20.clone.1 | output fusion | flops 133169152 | bytes 8388608 | tf_op jit(solution)/shard_map/reduce-window.4
  181.3 4.4 %copy.62 = f32[1,512,16,128]{1,3,2,0:T(8,128)} copy(f32[1,512,16,128]{1,2,3,0:T(8,128)S(1)} %fusion.71) | data formatting | bytes 8388608 | tf_op jit(solution)/shard_map/reduce-window.4
  185.9 7.0 %fusion.72 = bf16[512,2048]{0,1:T(8,128)(2,1)S(1)} fusion(f32[512,2048]{0,1:T(8,128)} %copy-done.1, f32[1,512,16,128]{1,3,2,0:T(8,128)} %copy.62, f32[2048,512]{1,0:T(8,128)} %get-tuple-element.236, f32[512]{0:T(512)S(1)} %bitcast.118, f32[512,16]{0,1:T(8,128)S(1)} %slice_bitcast_fusion.5, f32[2048]{0:T(1024)S(1)} %bitcast.117, s32[512]{0:T(512)S(1)} %fusion.69, ...), kind=kLoop, calls=%fused_computation.5.clone.1 | loop fusion | flops 17825792 | bytes 14733312 | tf_op jit(solution)/shard_map/while/body/convert_element_type | solution.py:88
  194.8 5.6 %fusion.70 = (f32[512]{0:T(512)S(1)}, f32[512,2048]{0,1:T(8,128)S(1)}, f32[2048,512]{1,0:T(8,128)}) fusion(f32[2048]{0:T(1024)S(1)} %bitcast.116, s32[512]{0:T(512)S(1)} %fusion.69, s32[2048]{0:T(1024)S(1)} %iota_add_fusion.2, bf16[1,512,128]{2,1,0:T(8,128)(2,1)S(1)} %get-tuple-element.274, bf16[16384,128]{1,0:T(8,128)(2,1)} %get-tuple-element.273, ...), kind=kOutput, calls=%fused_computation.73.clone.1 | convolution fusion | flops 281017856 | bytes 9064452 | tf_op jit(solution)/shard_map/while/body/grd,kgd->grk/dot_general | solution.py:80
  200.3 10.1 %fusion.71 = f32[1,512,16,128]{1,2,3,0:T(8,128)S(1)} fusion(f32[1,512,16,128]{1,3,2,0:T(8,128)S(1)} %bitcast.108), kind=kOutput, calls=%fused_computation.20.clone.1 | output fusion | flops 133169152 | bytes 8388608 | tf_op jit(solution)/shard_map/reduce-window.4
  210.4 4.4 %copy.62 = f32[1,512,16,128]{1,3,2,0:T(8,128)} copy(f32[1,512,16,128]{1,2,3,0:T(8,128)S(1)} %fusion.71) | data formatting | bytes 8388608 | tf_op jit(solution)/shard_map/reduce-window.4
  214.9 6.9 %fusion.72 = bf16[512,2048]{0,1:T(8,128)(2,1)S(1)} fusion(f32[512,2048]{0,1:T(8,128)} %copy-done.1, f32[1,512,16,128]{1,3,2,0:T(8,128)} %copy.62, f32[2048,512]{1,0:T(8,128)} %get-tuple-element.236, f32[512]{0:T(512)S(1)} %bitcast.118, f32[512,16]{0,1:T(8,128)S(1)} %slice_bitcast_fusion.5, f32[2048]{0:T(1024)S(1)} %bitcast.117, s32[512]{0:T(512)S(1)} %fusion.69, ...), kind=kLoop, calls=%fused_computation.5.clone.1 | loop fusion | flops 17825792 | bytes 14733312 | tf_op jit(solution)/shard_map/while/body/convert_element_type | solution.py:88
  221.9 1.8 fusion.73
  223.8 5.5 %fusion.70 = (f32[512]{0:T(512)S(1)}, f32[512,2048]{0,1:T(8,128)S(1)}, f32[2048,512]{1,0:T(8,128)}) fusion(f32[2048]{0:T(1024)S(1)} %bitcast.116, s32[512]{0:T(512)S(1)} %fusion.69, s32[2048]{0:T(1024)S(1)} %iota_add_fusion.2, bf16[1,512,128]{2,1,0:T(8,128)(2,1)S(1)} %get-tuple-element.274, bf16[16384,128]{1,0:T(8,128)(2,1)} %get-tuple-element.273, ...), kind=kOutput, calls=%fused_computation.73.clone.1 | convolution fusion | flops 281017856 | bytes 9064452 | tf_op jit(solution)/shard_map/while/body/grd,kgd->grk/dot_general | solution.py:80
  229.3 10.1 %fusion.71 = f32[1,512,16,128]{1,2,3,0:T(8,128)S(1)} fusion(f32[1,512,16,128]{1,3,2,0:T(8,128)S(1)} %bitcast.108), kind=kOutput, calls=%fused_computation.20.clone.1 | output fusion | flops 133169152 | bytes 8388608 | tf_op jit(solution)/shard_map/reduce-window.4
  239.4 4.4 %copy.62 = f32[1,512,16,128]{1,3,2,0:T(8,128)} copy(f32[1,512,16,128]{1,2,3,0:T(8,128)S(1)} %fusion.71) | data formatting | bytes 8388608 | tf_op jit(solution)/shard_map/reduce-window.4
  243.9 6.9 %fusion.72 = bf16[512,2048]{0,1:T(8,128)(2,1)S(1)} fusion(f32[512,2048]{0,1:T(8,128)} %copy-done.1, f32[1,512,16,128]{1,3,2,0:T(8,128)} %copy.62, f32[2048,512]{1,0:T(8,128)} %get-tuple-element.236, f32[512]{0:T(512)S(1)} %bitcast.118, f32[512,16]{0,1:T(8,128)S(1)} %slice_bitcast_fusion.5, f32[2048]{0:T(1024)S(1)} %bitcast.117, s32[512]{0:T(512)S(1)} %fusion.69, ...), kind=kLoop, calls=%fused_computation.5.clone.1 | loop fusion | flops 17825792 | bytes 14733312 | tf_op jit(solution)/shard_map/while/body/convert_element_type | solution.py:88
  250.8 1.8 fusion.73
  252.7 5.5 %fusion.70 = (f32[512]{0:T(512)S(1)}, f32[512,2048]{0,1:T(8,128)S(1)}, f32[2048,512]{1,0:T(8,128)}) fusion(f32[2048]{0:T(1024)S(1)} %bitcast.116, s32[512]{0:T(512)S(1)} %fusion.69, s32[2048]{0:T(1024)S(1)} %iota_add_fusion.2, bf16[1,512,128]{2,1,0:T(8,128)(2,1)S(1)} %get-tuple-element.274, bf16[16384,128]{1,0:T(8,128)(2,1)} %get-tuple-element.273, ...), kind=kOutput, calls=%fused_computation.73.clone.1 | convolution fusion | flops 281017856 | bytes 9064452 | tf_op jit(solution)/shard_map/while/body/grd,kgd->grk/dot_general | solution.py:80
  258.3 10.1 %fusion.71 = f32[1,512,16,128]{1,2,3,0:T(8,128)S(1)} fusion(f32[1,512,16,128]{1,3,2,0:T(8,128)S(1)} %bitcast.108), kind=kOutput, calls=%fused_computation.20.clone.1 | output fusion | flops 133169152 | bytes 8388608 | tf_op jit(solution)/shard_map/reduce-window.4
  268.4 4.4 %copy.62 = f32[1,512,16,128]{1,3,2,0:T(8,128)} copy(f32[1,512,16,128]{1,2,3,0:T(8,128)S(1)} %fusion.71) | data formatting | bytes 8388608 | tf_op jit(solution)/shard_map/reduce-window.4
  272.9 6.9 %fusion.72 = bf16[512,2048]{0,1:T(8,128)(2,1)S(1)} fusion(f32[512,2048]{0,1:T(8,128)} %copy-done.1, f32[1,512,16,128]{1,3,2,0:T(8,128)} %copy.62, f32[2048,512]{1,0:T(8,128)} %get-tuple-element.236, f32[512]{0:T(512)S(1)} %bitcast.118, f32[512,16]{0,1:T(8,128)S(1)} %slice_bitcast_fusion.5, f32[2048]{0:T(1024)S(1)} %bitcast.117, s32[512]{0:T(512)S(1)} %fusion.69, ...), kind=kLoop, calls=%fused_computation.5.clone.1 | loop fusion | flops 17825792 | bytes 14733312 | tf_op jit(solution)/shard_map/while/body/convert_element_type | solution.py:88
  279.8 1.8 fusion.73
  281.7 5.5 %fusion.70 = (f32[512]{0:T(512)S(1)}, f32[512,2048]{0,1:T(8,128)S(1)}, f32[2048,512]{1,0:T(8,128)}) fusion(f32[2048]{0:T(1024)S(1)} %bitcast.116, s32[512]{0:T(512)S(1)} %fusion.69, s32[2048]{0:T(1024)S(1)} %iota_add_fusion.2, bf16[1,512,128]{2,1,0:T(8,128)(2,1)S(1)} %get-tuple-element.274, bf16[16384,128]{1,0:T(8,128)(2,1)} %get-tuple-element.273, ...), kind=kOutput, calls=%fused_computation.73.clone.1 | convolution fusion | flops 281017856 | bytes 9064452 | tf_op jit(solution)/shard_map/while/body/grd,kgd->grk/dot_general | solution.py:80
  287.2 10.1 %fusion.71 = f32[1,512,16,128]{1,2,3,0:T(8,128)S(1)} fusion(f32[1,512,16,128]{1,3,2,0:T(8,128)S(1)} %bitcast.108), kind=kOutput, calls=%fused_computation.20.clone.1 | output fusion | flops 133169152 | bytes 8388608 | tf_op jit(solution)/shard_map/reduce-window.4
  297.3 4.4 %copy.62 = f32[1,512,16,128]{1,3,2,0:T(8,128)} copy(f32[1,512,16,128]{1,2,3,0:T(8,128)S(1)} %fusion.71) | data formatting | bytes 8388608 | tf_op jit(solution)/shard_map/reduce-window.4
  301.8 6.9 %fusion.72 = bf16[512,2048]{0,1:T(8,128)(2,1)S(1)} fusion(f32[512,2048]{0,1:T(8,128)} %copy-done.1, f32[1,512,16,128]{1,3,2,0:T(8,128)} %copy.62, f32[2048,512]{1,0:T(8,128)} %get-tuple-element.236, f32[512]{0:T(512)S(1)} %bitcast.118, f32[512,16]{0,1:T(8,128)S(1)} %slice_bitcast_fusion.5, f32[2048]{0:T(1024)S(1)} %bitcast.117, s32[512]{0:T(512)S(1)} %fusion.69, ...), kind=kLoop, calls=%fused_computation.5.clone.1 | loop fusion | flops 17825792 | bytes 14733312 | tf_op jit(solution)/shard_map/while/body/convert_element_type | solution.py:88
  308.8 1.8 fusion.73
  310.7 5.5 %fusion.70 = (f32[512]{0:T(512)S(1)}, f32[512,2048]{0,1:T(8,128)S(1)}, f32[2048,512]{1,0:T(8,128)}) fusion(f32[2048]{0:T(1024)S(1)} %bitcast.116, s32[512]{0:T(512)S(1)} %fusion.69, s32[2048]{0:T(1024)S(1)} %iota_add_fusion.2, bf16[1,512,128]{2,1,0:T(8,128)(2,1)S(1)} %get-tuple-element.274, bf16[16384,128]{1,0:T(8,128)(2,1)} %get-tuple-element.273, ...), kind=kOutput, calls=%fused_computation.73.clone.1 | convolution fusion | flops 281017856 | bytes 9064452 | tf_op jit(solution)/shard_map/while/body/grd,kgd->grk/dot_general | solution.py:80
  316.2 10.1 %fusion.71 = f32[1,512,16,128]{1,2,3,0:T(8,128)S(1)} fusion(f32[1,512,16,128]{1,3,2,0:T(8,128)S(1)} %bitcast.108), kind=kOutput, calls=%fused_computation.20.clone.1 | output fusion | flops 133169152 | bytes 8388608 | tf_op jit(solution)/shard_map/reduce-window.4
  326.3 4.4 %copy.62 = f32[1,512,16,128]{1,3,2,0:T(8,128)} copy(f32[1,512,16,128]{1,2,3,0:T(8,128)S(1)} %fusion.71) | data formatting | bytes 8388608 | tf_op jit(solution)/shard_map/reduce-window.4
  330.8 6.9 %fusion.72 = bf16[512,2048]{0,1:T(8,128)(2,1)S(1)} fusion(f32[512,2048]{0,1:T(8,128)} %copy-done.1, f32[1,512,16,128]{1,3,2,0:T(8,128)} %copy.62, f32[2048,512]{1,0:T(8,128)} %get-tuple-element.236, f32[512]{0:T(512)S(1)} %bitcast.118, f32[512,16]{0,1:T(8,128)S(1)} %slice_bitcast_fusion.5, f32[2048]{0:T(1024)S(1)} %bitcast.117, s32[512]{0:T(512)S(1)} %fusion.69, ...), kind=kLoop, calls=%fused_computation.5.clone.1 | loop fusion | flops 17825792 | bytes 14733312 | tf_op jit(solution)/shard_map/while/body/convert_element_type | solution.py:88
  337.7 1.8 fusion.73
  340.8 19.6 %all_to_all.21 = bf16[4,256,512]{2,1,0:T(8,128)(2,1)S(1)} all-to-all(bf16[4,256,512]{2,1,0:T(8,128)(2,1)S(1)} %bitcast.112), channel_id=1, replica_groups=mesh['sp'=64,'tp'=4] {'tp'}, dimensions={0} | all-to-all | bytes 2097152 | tf_op jit(solution)/shard_map/all_to_all | solution.py:34
  361.3 3.2 all-to-all-start.1
  365.3 4.5 %all-to-all-done.1 = f32[4,1,256]{2,1,0:T(1,128)S(1)} async-done(((f32[4,1,256]{2,1,0:T(1,128)}), f32[4,1,256]{2,1,0:T(1,128)S(1)}, u32[]{:S(2)}, u32[]{:S(2)}) %all-to-all-start.1) | async-done | bytes 4128 | tf_op jit(solution)/shard_map/all_to_all | solution.py:40
  370.2 15.9 %all_to_all.22 = bf16[4,256,512]{1,2,0:T(8,128)(2,1)S(1)} all-to-all(bf16[4,256,512]{1,2,0:T(8,128)(2,1)S(1)} %broadcast_in_dim.18), channel_id=1, replica_groups=mesh['sp'=64,'tp'=4] {'tp'}, dimensions={0} | all-to-all | bytes 2097152 | tf_op jit(solution)/shard_map/all_to_all | solution.py:40
  386.1 10.3 %fusion.39 = bf16[256,2048]{1,0:T(8,128)(2,1)S(1)} fusion(bf16[2048,4096]{1,0:T(8,128)(2,1)} %all-gather.5.cloned.1.call-done, bf16[256,2048]{0,1:T(8,128)(2,1)S(1)} %bitcast.114), kind=kOutput, calls=%fused_computation.50 | convolution fusion | flops 4297064448 | bytes 18874368 | tf_op jit(solution)/shard_map/dot_general | solution.py:143
  396.5 15.1 %all_to_all.23 = bf16[4,256,512]{2,1,0:T(8,128)(2,1)S(1)} all-to-all(bf16[4,256,512]{2,1,0:T(8,128)(2,1)S(1)} %bitcast.113), channel_id=1, replica_groups=mesh['sp'=64,'tp'=4] {'tp'}, dimensions={0} | all-to-all | bytes 2097152 | tf_op jit(solution)/shard_map/all_to_all | solution.py:34
  (111 shorter events, 14.1 us)
Async XLA Ops:
  6.5 333.7 %copy-start = (bf16[256,2048]{1,0:T(8,128)(2,1)S(1)}, bf16[256,2048]{1,0:T(8,128)(2,1)}, u32[]{:S(2)}) copy-start(bf16[256,2048]{1,0:T(8,128)(2,1)} %param.18) | copy-start | bytes 3145732
  6.5 92.0 %all-gather.3.cloned.1.call-start = ((), (), s32[]{:S(2)}) async-start(), calls=%async_computation.4 | async-start | bytes 12779520 | tf_op jit(solution)/shard_map/all_gather | solution.py:16
  9.0 377.0 %all-gather.5.cloned.1.call-start = ((), (), s32[]{:S(2)}) async-start(), calls=%async_computation.5 | async-start | bytes 17039360 | tf_op jit(solution)/shard_map/all_gather | solution.py:16
  107.3 232.7 %copy-start.3 = (f32[256]{0:T(256)S(1)}, f32[256]{0:T(256)}, u32[]{:S(2)}) copy-start(f32[256]{0:T(256)} %param.17) | copy-start | bytes 3076
  113.0 10.1 %copy-start.1 = (f32[512,2048]{0,1:T(8,128)}, f32[512,2048]{0,1:T(8,128)S(1)}, u32[]{:S(2)}) copy-start(f32[512,2048]{0,1:T(8,128)S(1)} %get-tuple-element.235) | copy-start | bytes 12582916 | tf_op jit(solution)/shard_map/while
  142.0 10.1 %copy-start.1 = (f32[512,2048]{0,1:T(8,128)}, f32[512,2048]{0,1:T(8,128)S(1)}, u32[]{:S(2)}) copy-start(f32[512,2048]{0,1:T(8,128)S(1)} %get-tuple-element.235) | copy-start | bytes 12582916 | tf_op jit(solution)/shard_map/while
  171.2 10.1 %copy-start.1 = (f32[512,2048]{0,1:T(8,128)}, f32[512,2048]{0,1:T(8,128)S(1)}, u32[]{:S(2)}) copy-start(f32[512,2048]{0,1:T(8,128)S(1)} %get-tuple-element.235) | copy-start | bytes 12582916 | tf_op jit(solution)/shard_map/while
  200.3 10.1 %copy-start.1 = (f32[512,2048]{0,1:T(8,128)}, f32[512,2048]{0,1:T(8,128)S(1)}, u32[]{:S(2)}) copy-start(f32[512,2048]{0,1:T(8,128)S(1)} %get-tuple-element.235) | copy-start | bytes 12582916 | tf_op jit(solution)/shard_map/while
  229.3 10.1 %copy-start.1 = (f32[512,2048]{0,1:T(8,128)}, f32[512,2048]{0,1:T(8,128)S(1)}, u32[]{:S(2)}) copy-start(f32[512,2048]{0,1:T(8,128)S(1)} %get-tuple-element.235) | copy-start | bytes 12582916 | tf_op jit(solution)/shard_map/while
  258.3 10.1 %copy-start.1 = (f32[512,2048]{0,1:T(8,128)}, f32[512,2048]{0,1:T(8,128)S(1)}, u32[]{:S(2)}) copy-start(f32[512,2048]{0,1:T(8,128)S(1)} %get-tuple-element.235) | copy-start | bytes 12582916 | tf_op jit(solution)/shard_map/while
  287.2 10.1 %copy-start.1 = (f32[512,2048]{0,1:T(8,128)}, f32[512,2048]{0,1:T(8,128)S(1)}, u32[]{:S(2)}) copy-start(f32[512,2048]{0,1:T(8,128)S(1)} %get-tuple-element.235) | copy-start | bytes 12582916 | tf_op jit(solution)/shard_map/while
  316.2 10.1 %copy-start.1 = (f32[512,2048]{0,1:T(8,128)}, f32[512,2048]{0,1:T(8,128)S(1)}, u32[]{:S(2)}) copy-start(f32[512,2048]{0,1:T(8,128)S(1)} %get-tuple-element.235) | copy-start | bytes 12582916 | tf_op jit(solution)/shard_map/while
  340.1 20.5 %copy-start.2 = (bf16[256,512]{1,0:T(8,128)(2,1)S(1)}, bf16[256,512]{1,0:T(8,128)(2,1)}, u32[]{:S(2)}) copy-start(bf16[256,512]{1,0:T(8,128)(2,1)} %param.12) | copy-start | bytes 786436
  361.3 8.5 %all-to-all-start.1 = ((f32[4,1,256]{2,1,0:T(1,128)}), f32[4,1,256]{2,1,0:T(1,128)S(1)}, u32[]{:S(2)}, u32[]{:S(2)}) async-start(f32[4,1,256]{2,1,0:T(1,128)} %broadcast_in_dim.17), calls=%async_computation.1 | async-start | bytes 8192 | tf_op jit(solution)/shard_map/all_to_all | solution.py:40
Sparse Core Ops, SparseCore 0:
  10.1 88.3 all-gather.2
  101.3 95.6 all-gather.4
where the time goes:
time: 420 us; the launch traced here: 419 us
  other arithmetic  142 us (34%)
  waiting for transfers between devices  91.2 us (22%)
  matrix products  69.4 us (17%)
  blocking collectives  50.6 us (12%)
  local copies, waits for them, and re-layouts  47.9 us (11%)
  between operations  13.6 us (3%)
    all_gather x2, waiting for transfers between devices, turned_gather(): result = lax.all_gather(both, axis, axis=0, tiled=True)  86.7 us
    another operation x16, other arithmetic  81.4 us
    convert_element_type x8, other arithmetic, one_block(): jnp.where(visible, jnp.exp(jax.nn.log_sigmoid(scores) + later), 0.0)  55.7 us
    dot_general x8, matrix products, one_block(): jnp.einsum('grd,kgd->grk', stacked, key_block_rows, preferred_element_typ...  44.3 us
    another operation x24, local copies, waits for them, and re-layouts  35.3 us
    all_to_all x2, blocking collectives, sent_and_summed(): pieces = lax.all_to_all(in_blocks(array, dim, size), axis, 0, 0, tiled=True)  34.7 us
    all_to_all x1, blocking collectives, sent_to_all(): lax.all_to_all(jnp.broadcast_to(array[None], (size, *array.shape)), axis,...  15.9 us
    dot_general x8, matrix products, one_block(): jnp.einsum('grk,kgd->grd', weights, value_block_rows, preferred_element_t...  14.4 us
  transfers between devices with their start and end apart: 3, of which 2 were waited for; matrix products, arithmetic and copies ran while one was open for 59% of the time, Pallas kernels for 0%

commit v1 on v0

v1 whole, which is shorter than its diff:
```python
import functools
import math

import jax
import jax.numpy as jnp
from jax import lax
from jax.experimental import pallas as pl
from jax.experimental.pallas import tpu as pltpu
from jax.sharding import PartitionSpec as P

MESH = pl.DeviceIdType.MESH
HEAD_DIM = 128
EPS = 1e-06
LOG2E = 1.4426950408889634
SCALE2 = LOG2E / math.sqrt(HEAD_DIM)
NT = (((1,), (1,)), ((), ()))
F32 = jnp.float32
BF16 = jnp.bfloat16
KV_SUBS = 2
W_SUBS = 4
STEPS = 16


def ring_one_position(x, z):
    return 4 * z + lax.rem(x + z, 4)


def ring_one_chip(p):
    row = lax.div(p, 4)
    return 4 * row + lax.rem(p + 3 * row, 4)


def ring_two_position(x, z):
    d = lax.rem(z + 5 * x, 8)
    return 4 * x + d + 12 * lax.div(d, 4)


def ring_two_chip(p):
    seg = lax.div(p, 4)
    return 4 * lax.rem(3 * seg + lax.rem(p, 4), 8) + lax.rem(seg, 4)


def kernel(
    res_ref, q_ref, k_ref, v_ref, gain_ref, ow_ref, mg_ref, up_ref, dn_ref, out_ref,
    kg, vg, upg, dng, owg, resg, attg, qs, acc, carry, hid, mi, act, rs_out, rs_in, own_part,
    kv_recv, w_recv, kv_send, w_send, kv_pair_send, kv_pair_recv, w_pair_send, w_pair_recv,
    local_sem, ow_send, ow_recv, ow_pair_send, ow_pair_recv, res_send, res_recv,
    att_send, att_recv, rs_send, rs_recv,
):
    sp = lax.axis_index("sp")
    tp = lax.axis_index("tp")
    core = lax.rem(sp, 2)
    chip = lax.div(sp, 2)
    x, z = lax.rem(chip, 4), lax.div(chip, 4)
    partner = (sp + 1 - 2 * core, tp)
    p1, p2 = ring_one_position(x, z), ring_two_position(x, z)

    def on_ring(ring, p):
        return 2 * (ring_one_chip(p) if ring == 0 else ring_two_chip(p)) + core

    here = (p1, p2)
    nxt = [(on_ring(r, lax.rem(here[r] + 1, 32)), tp) for r in (0, 1)]
    prv = [(on_ring(r, lax.rem(here[r] + 31, 32)), tp) for r in (0, 1)]
    target = (nxt[0], prv[0], nxt[1], prv[1])
    peers = [(sp, lax.rem(tp + d, 4)) for d in (1, 2, 3)]
    everyone = [nxt[0], prv[0], nxt[1], prv[1], partner] + peers

    barrier = pltpu.get_barrier_semaphore()
    for device in everyone:
        pl.semaphore_signal(barrier, inc=1, device_id=device, device_id_type=MESH)
    pl.semaphore_wait(barrier, len(everyone))

    def remote(src, dst, send_sem, recv_sem, device):
        return pltpu.make_async_remote_copy(
            src_ref=src, dst_ref=dst, send_sem=send_sem, recv_sem=recv_sem,
            device_id=device, device_id_type=MESH,
        )

    def waits(ref, sem):
        pltpu.make_async_copy(ref, ref, sem).wait()

    def kv_slot(ring, origin, sub):
        return (kg if ring == 0 else vg).at[origin * KV_SUBS + sub]

    def w_slot(ring, origin, sub):
        rows = pl.ds(pl.multiple_of(origin * 32, 32), 32)
        return (upg if ring == 0 else dng).at[sub, rows, :]

    for sub in range(KV_SUBS):
        for j in range(4):
            ring = j // 2
            src = (k_ref if ring == 0 else v_ref).at[sub]
            remote(src, kv_slot(ring, sp, sub), kv_send.at[j], kv_recv.at[j, sub], target[j]).start()
    for sub in range(W_SUBS):
        for j in range(4):
            ring = j // 2
            src = (up_ref if ring == 0 else dn_ref).at[:, pl.ds(sub * 512, 512)]
            remote(src, w_slot(ring, sp, sub), w_send.at[j], w_recv.at[j, sub], target[j]).start()
    half = pl.ds(pl.multiple_of(core * 1024, 1024), 1024)
    for d in (1, 2, 3):
        remote(res_ref, resg.at[tp], res_send.at[d - 1], res_recv.at[d - 1], peers[d - 1]).start()
    for d in (1, 2, 3):
        remote(
            ow_ref.at[:, half], owg.at[tp, core], ow_send.at[d - 1], ow_recv.at[d - 1], peers[d - 1]
        ).start()
    locals_ = []

    def keep(src, dst):
        copy = pltpu.make_async_copy(src, dst, local_sem.at[len(locals_)])
        copy.start()
        locals_.append(copy)

    for ring in (0, 1):
        for sub in range(KV_SUBS):
            src = (k_ref if ring == 0 else v_ref).at[sub]
            remote(
                src, kv_slot(ring, sp, sub), kv_pair_send.at[ring], kv_pair_recv.at[ring], partner
            ).start()
            keep(src, kv_slot(ring, sp, sub))
        for sub in range(W_SUBS):
            src = (up_ref if ring == 0 else dn_ref).at[:, pl.ds(sub * 512, 512)]
            remote(
                src, w_slot(ring, sp, sub), w_pair_send.at[ring], w_pair_recv.at[ring], partner
            ).start()
            keep(src, w_slot(ring, sp, sub))
    for c in range(2):
        keep(ow_ref.at[:, pl.ds(c * 1024, 1024)], owg.at[tp, c])
    keep(res_ref, resg.at[tp])
    qs[0:256, :] = q_ref[:, 0:128]
    qs[256:512, :] = q_ref[:, 128:256]

    def ring_step(n, subs, slot, send, recv, pair_send, pair_recv):
        s = lax.div(n, subs) + 1
        sub = lax.rem(n, subs)
        for j in range(4):
            ring, back = j // 2, j % 2
            last = STEPS - back
            p = here[ring]
            origin = on_ring(ring, lax.rem(p + s, 32) if back else lax.rem(p + 32 - s, 32))
            block = slot(ring, origin, sub)

            @pl.when(s <= last)
            def _():
                remote(block, block, send.at[j], recv.at[j, n], target[j]).wait_recv()

            @pl.when(s < last)
            def _():
                remote(block, block, send.at[j], recv.at[j, n + subs], target[j]).start()

            @pl.when(s <= last)
            def _():
                remote(block, block, pair_send.at[ring], pair_recv.at[ring], partner).start()

    def kv_step(n):
        ring_step(n, KV_SUBS, kv_slot, kv_send, kv_recv, kv_pair_send, kv_pair_recv)

    def w_step(n):
        ring_step(n, W_SUBS, w_slot, w_send, w_recv, w_pair_send, w_pair_recv)

    kv_total, w_total = STEPS * KV_SUBS, STEPS * W_SUBS

    def gather_keys(n, _):
        kv_step(n)
        w_step(n)
        return 0

    lax.fori_loop(0, kv_total, gather_keys, 0)
    for ring in (0, 1):
        buf = kg if ring == 0 else vg
        waits(buf.at[0:64], kv_pair_recv.at[ring])
    for copy in locals_:
        copy.wait()

    row = lax.broadcasted_iota(jnp.int32, (256, 256), 0)
    col = lax.broadcasted_iota(jnp.int32, (256, 256), 1)
    later_keys = (row > col).astype(BF16)
    acc[...] = jnp.zeros_like(acc)
    carry[...] = jnp.zeros_like(carry)

    def attend(block, diagonal):
        both = pl.ds(pl.multiple_of(block * 2, 2), 2)
        keys = kg[both, 0:128, :].reshape(256, 128)
        values = vg[both, :, :].reshape(256, 128)
        shift = kg[both, 128:144, :].astype(F32) * LOG2E
        shift = jnp.concatenate([shift[0, 0:1, :], shift[1, 0:1, :]], axis=1)
        t = lax.dot_general(qs[...], keys, NT, preferred_element_type=F32) * SCALE2 + shift
        soft = jnp.maximum(t, jnp.log2(1.0 + jnp.exp2(jnp.minimum(t, 126.0))))
        broken = soft
        if diagonal:
            q_pos = lax.rem(lax.broadcasted_iota(jnp.int32, (512, 256), 0), 256)
            visible = lax.broadcasted_iota(jnp.int32, (512, 256), 1) < q_pos
            broken = jnp.where(visible, soft, 0.0)
        later = jnp.dot(broken.astype(BF16), later_keys, preferred_element_type=F32)
        after = carry[...]
        weights = jnp.exp2((t - soft) - (later + after))
        if diagonal:
            weights = jnp.where(visible, weights, 0.0)
        acc[...] += jnp.dot(weights.astype(BF16), values, preferred_element_type=F32)
        carry[...] = after + (later[:, 0:1] + broken[:, 0:1])

    attend(sp, True)

    def beside_weights(n, _):
        w_step(n)
        block = sp - 1 - (n - kv_total)

        @pl.when(block >= 0)
        def _():
            attend(jnp.maximum(block, 0), False)

        return 0

    lax.fori_loop(kv_total, w_total, beside_weights, 0)
    for d in (1, 2, 3):
        source = lax.rem(tp + 4 - d, 4)
        block = owg.at[source, core]
        remote(block, block, ow_send.at[d - 1], ow_recv.at[d - 1], partner).wait_recv()
        remote(block, block, ow_pair_send, ow_pair_recv, partner).start()
    done = w_total - kv_total
    lax.fori_loop(
        done, jnp.maximum(sp, done), lambda n, _: (attend(sp - 1 - n, False), 0)[1], 0
    )

    for h in range(2):
        mixed = acc[pl.ds(h * 256, 256), :]
        power = jnp.mean(mixed * mixed, axis=1, keepdims=True)
        lanes = slice(h * 128, h * 128 + 128)
        attg[tp, :, lanes] = (mixed * lax.rsqrt(power + EPS) * gain_ref[0:1, lanes]).astype(BF16)
    for d in (2, 1, 3):
        remote(
            attg.at[tp], attg.at[tp], att_send.at[d - 1], att_recv.at[d - 1], peers[d - 1]
        ).start()
    waits(owg.at[0:3, 0], ow_pair_recv)
    for d in (1, 2, 3):
        block = resg.at[tp]
        remote(block, block, res_send.at[d - 1], res_recv.at[d - 1], peers[d - 1]).wait_recv()
    for d in (1, 2, 3):
        block = attg.at[tp]
        remote(block, block, att_send.at[d - 1], att_recv.at[d - 1], peers[d - 1]).wait_recv()

    squares = jnp.zeros((256, 1), F32)
    for b in range(4):
        total = resg[b].astype(F32)
        for g in range(4):
            weight = owg[g, b // 2, :, (b % 2) * 512 : (b % 2) * 512 + 512]
            total = total + jnp.dot(attg[g], weight, preferred_element_type=F32)
        hidden = total.astype(BF16)
        hid[b] = hidden
        wide = hidden.astype(F32)
        squares = squares + jnp.sum(wide * wide, axis=1, keepdims=True)
    inverse = lax.rsqrt(squares / 2048.0 + EPS)
    for b in range(4):
        mi[:, b * 512 : b * 512 + 512] = (hid[b].astype(F32) * inverse * mg_ref[b]).astype(BF16)

    waits(upg.at[0:2], w_pair_recv.at[0])
    waits(dng.at[0:2], w_pair_recv.at[1])
    for b in range(4):
        lifted = jnp.dot(mi[...], upg[b], preferred_element_type=F32)
        lifted = jnp.maximum(lifted, 0.0)
        act[b] = (lifted * lifted).astype(BF16)

    def down(owner):
        rows = pl.ds(pl.multiple_of(owner * 512, 512), 512)
        total = jnp.zeros((256, 512), F32)
        for b in range(4):
            total = total + lax.dot_general(
                act[b], dng[b, rows, :], NT, preferred_element_type=F32
            )
        return total

    for d in (2, 1, 3):
        rs_out[d - 1] = down(lax.rem(tp + d, 4)).astype(BF16)
        remote(
            rs_out.at[d - 1], rs_in.at[d - 1], rs_send.at[d - 1], rs_recv.at[d - 1], peers[d - 1]
        ).start()
    own_part[...] = down(tp) + hid[tp].astype(F32)
    for d in (1, 3, 2):
        remote(
            rs_out.at[d - 1], rs_in.at[d - 1], rs_send.at[d - 1], rs_recv.at[d - 1], peers[d - 1]
        ).wait_recv()
    out_ref[...] = (
        own_part[...] + rs_in[0].astype(F32) + rs_in[1].astype(F32) + rs_in[2].astype(F32)
    ).astype(BF16)

    for j in range(4):
        ring, back = j // 2, j % 2
        waits((kg if ring == 0 else vg).at[0 : 32 - 2 * back], kv_send.at[j])
        waits((upg if ring == 0 else dng).at[0, 0 : 2048 - 128 * back, :], w_send.at[j])
    for ring in (0, 1):
        waits((kg if ring == 0 else vg).at[0:64], kv_pair_send.at[ring])
        waits((upg if ring == 0 else dng).at[0:2], w_pair_send.at[ring])
    waits(owg.at[0:3, 0], ow_pair_send)
    for d in (1, 2, 3):
        waits(res_ref, res_send.at[d - 1])
        waits(owg.at[0, 0], ow_send.at[d - 1])
        waits(attg.at[0], att_send.at[d - 1])
        waits(rs_out.at[d - 1], rs_send.at[d - 1])


def body(
    residual, queries, key_rows, value_rows, break_shift, head_gain, out_weight, mlp_gain,
    up_weight, down_weight,
):
    shift = jnp.pad(break_shift.reshape(2, 1, 128), ((0, 0), (0, 15), (0, 0)))
    keys = jnp.concatenate([key_rows.reshape(2, 128, 128), shift], axis=1)
    values = value_rows.reshape(2, 128, 128)
    vmem = pltpu.VMEM
    dma = pltpu.SemaphoreType.DMA
    return pl.pallas_call(
        kernel,
        out_shape=jax.ShapeDtypeStruct((256, 512), BF16),
        in_specs=[pl.BlockSpec(memory_space=vmem)] * 9,
        out_specs=pl.BlockSpec(memory_space=vmem),
        scratch_shapes=[
            vmem((128, 144, 128), BF16),
            vmem((128, 128, 128), BF16),
            vmem((4, 2048, 512), BF16),
            vmem((4, 2048, 512), BF16),
            vmem((4, 2, 256, 1024), BF16),
            vmem((4, 256, 512), BF16),
            vmem((4, 256, 256), BF16),
            vmem((512, 128), BF16),
            vmem((512, 128), F32),
            vmem((512, 1), F32),
            vmem((4, 256, 512), BF16),
            vmem((256, 2048), BF16),
            vmem((4, 256, 512), BF16),
            vmem((3, 256, 512), BF16),
            vmem((3, 256, 512), BF16),
            vmem((256, 512), F32),
            dma((4, STEPS * KV_SUBS)),
            dma((4, STEPS * W_SUBS)),
            dma((4,)),
            dma((4,)),
            dma((2,)),
            dma((2,)),
            dma((2,)),
            dma((2,)),
            dma((15,)),
            dma((3,)),
            dma((3,)),
            dma,
            dma,
            dma((3,)),
            dma((3,)),
            dma((3,)),
            dma((3,)),
            dma((3,)),
            dma((3,)),
        ],
        compiler_params=pltpu.CompilerParams(
            collective_id=0, has_side_effects=True, vmem_limit_bytes=60 * 1024 * 1024
        ),
        name="layer",
    )(
        residual, queries, keys, values, head_gain.reshape(1, 256), out_weight,
        mlp_gain.reshape(4, 1, 512), up_weight, down_weight.T,
    )


def solution(mesh):
    in_specs = (
        P("sp", "tp"),
        P("sp", "tp"),
        P("sp", "tp"),
        P("sp", "tp"),
        P("tp", "sp"),
        P("tp"),
        P("tp", None),
        P(),
        P("sp", "tp"),
        P("tp", "sp"),
    )
    return jax.shard_map(
        body, mesh=mesh, in_specs=in_specs, out_specs=P("sp", "tp"), check_vma=False
    )
```

time: 420 us -> 144 us (0.34)
  the two profiles are of different devices: /device:TPU:224 before, /device:TPU:231 now
where the time goes in v1:
time: 144 us
  Pallas kernels  140 us (97%)
  local copies, waits for them, and re-layouts  2.35 us (2%)
  other arithmetic  1.48 us (1%)
    pallas_call x1, Pallas kernels, body(): pl.pallas_call(kernel, out_shape=jax.ShapeDtypeStruct((256, 512), BF16),...  140 us

profile of v1, /device:TPU:231, one launch (start us, length us, event | category | flops | bytes accessed | tf_op | source)
XLA Modules:
  0.0 143.7 jit_solution(11690841162678318711)
XLA Ops:
  0.0 0.0 copy-start
  0.0 0.7 copy-done
  0.7 1.5 %fusion.1.k_ref = bf16[2,144,128]{2,1,0:T(8,128)(2,1)} fusion(bf16[2,1,128]{2,1,0:T(2,128)(2,1)S(1)} %bitcast.10, bf16[2,128,128]{2,1,0:T(8,128)(2,1)} %bitcast.7), kind=kLoop, calls=%fused_computation.2 | loop fusion | flops 221184 | bytes 139776 | tf_op jit(solution)/shard_map/concatenate | solution.py:305
  2.2 139.9 %layer.1 = bf16[256,512]{1,0:T(8,128)(2,1)} custom-call(bf16[256,512]{1,0:T(8,128)(2,1)} %res_ref.1, bf16[256,256]{1,0:T(8,128)(2,1)} %q_ref.1, bf16[2,144,128]{2,1,0:T(8,128)(2,1)} %fusion.1.k_ref, bf16[2,128,128]{2,1,0:T(8,128)(2,1)} %bitcast.8, f32[1,256]{1,0:T(1,128)} %bitcast.11, bf16[256,2048]{1,0:T(8,128)(2,1)} %ow_ref.1, f32[4,1,512]{2,1,0:T(1,128)} %bitcast.9, ...), custom_call_target="tpu_custom_call" | custom-call | tf_op jit(solution)/shard_map/layer/pallas_call | solution.py:309
  142.1 1.7 %copy.12 = bf16[256,512]{1,0:T(8,128)(2,1)} copy(bf16[256,512]{1,0:T(8,128)(2,1)} %layer.1) | data formatting | bytes 524288
Async XLA Ops:
  0.0 0.7 copy-start

commit v2 on v1

v2 whole, which is shorter than its diff:
```python
import functools
import math

import jax
import jax.numpy as jnp
from jax import lax
from jax.experimental import pallas as pl
from jax.experimental.pallas import tpu as pltpu
from jax.sharding import PartitionSpec as P

MESH = pl.DeviceIdType.MESH
HEAD_DIM = 128
EPS = 1e-06
LOG2E = 1.4426950408889634
SCALE2 = LOG2E / math.sqrt(HEAD_DIM)
NT = (((1,), (1,)), ((), ()))
F32 = jnp.float32
BF16 = jnp.bfloat16
KV_ROWS = 528
KV_PIECES = 3
KV_PIECE = KV_ROWS // KV_PIECES
UP_PIECES = 3
DOWN_PIECES = 5
X_SIZE, Z_SIZE = 4, 8


def offset_of(k, size):
    return jnp.where(lax.rem(k, 2) == 1, lax.div(k + 1, 2), lax.rem(size - lax.div(k, 2), size))


def last_step(size, direction, even):
    return size // 2 - jnp.where(even == (direction == 0), 0, 1)


def kernel(
    res_ref, q_ref, kv_ref, gain_ref, ow_ref, mg_ref, up_ref, dn_ref, out_ref,
    kvg, wg, owg, resg, attg, qg, part, total_out, part_in, total_in, acc, carry, hid, mi, act, rs_out, rs_in, own_part,
    row_recv, side_recv, kv_send, kv_pair_send, kv_pair_recv, q_send, q_recv,
    part_send, part_recv, total_send, total_recv,
    ua_recv, um_recv, da_recv, dm_recv, gather_send, pair_send, pair_recv,
    local_sem, ow_send, ow_recv, ow_pair_send, ow_pair_recv, res_send, res_recv,
    att_send, att_recv, rs_send, rs_recv,
):
    sp = lax.axis_index("sp")
    tp = lax.axis_index("tp")
    core = lax.rem(sp, 2)
    chip = lax.div(sp, 2)
    x, z = lax.rem(chip, 4), lax.div(chip, 4)
    partner = (sp + 1 - 2 * core, tp)

    def device_at(x, z):
        return 2 * (X_SIZE * z + x) + core

    x_sides = [(device_at(lax.rem(x + d, X_SIZE), z), tp) for d in (1, X_SIZE - 1)]
    z_sides = [(device_at(x, lax.rem(z + d, Z_SIZE)), tp) for d in (1, Z_SIZE - 1)]
    peers = [(sp, lax.rem(tp + d, 4)) for d in (1, 2, 3)]
    below = [(device_at(x, lax.rem(z + Z_SIZE - 2 * (i + 1), Z_SIZE)), tp) for i in range(3)]
    everyone = x_sides + z_sides + [partner] + below + peers

    barrier = pltpu.get_barrier_semaphore()
    for device in everyone:
        pl.semaphore_signal(barrier, inc=1, device_id=device, device_id_type=MESH)
    pl.semaphore_wait(barrier, len(everyone))

    def remote(src, dst, send_sem, recv_sem, device):
        return pltpu.make_async_remote_copy(
            src_ref=src, dst_ref=dst, send_sem=send_sem, recv_sem=recv_sem,
            device_id=device, device_id_type=MESH,
        )

    def waits(ref, sem):
        pltpu.make_async_copy(ref, ref, sem).wait()

    def w_slot(first):
        def slot(origin, piece):
            return wg.at[first + piece, pl.ds(pl.multiple_of(origin * 32, 32), 32), :]

        return slot

    def w_source(page):
        ref, block = (dn_ref, page) if page < 4 else (up_ref, (3, 0, 1, 2)[page - 4])
        return ref.at[:, pl.ds(block * 512, 512)]

    class Gather:
        def __init__(self, number, x_first, pieces, slot, sources, first_recv, main_recv, pair):
            self.x_first, self.pieces, self.slot, self.sources = x_first, pieces, slot, sources
            self.first_recv, self.main_recv, self.pair = first_recv, main_recv, pair
            self.first_size, self.main_size = (X_SIZE, Z_SIZE) if x_first else (Z_SIZE, X_SIZE)
            self.first_to, self.main_to = (x_sides, z_sides) if x_first else (z_sides, x_sides)
            self.sem = lambda phase, d: gather_send.at[number * 4 + phase * 2 + d]

        def origin(self, first, main):
            first_at, main_at = (x, z) if self.x_first else (z, x)
            a = lax.rem(first_at + first, self.first_size)
            b = lax.rem(main_at + main, self.main_size)
            return device_at(a, b) if self.x_first else device_at(b, a)

        def send_first(self, src, dst, d, step, piece):
            return remote(
                src, dst, self.sem(0, d), self.first_recv.at[d, step - 1, piece], self.first_to[d]
            )

        def send_main(self, src, dst, d, step, k, piece):
            return remote(
                src, dst, self.sem(1, d), self.main_recv.at[d, step - 1, k, piece], self.main_to[d]
            )

        def to_partner(self, src, dst):
            remote(src, dst, pair_send.at[self.pair], pair_recv.at[self.pair], partner).start()

        def own(self):
            for piece in range(self.pieces):
                src, dst = self.sources[piece], self.slot(sp, piece)
                for d in range(2):
                    self.send_first(src, dst, d, 1, piece).start()
            for piece in range(self.pieces):
                src, dst = self.sources[piece], self.slot(sp, piece)
                for d in range(2):
                    self.send_main(src, dst, d, 1, 0, piece).start()

        def own_near(self):
            for piece in range(self.pieces):
                src, dst = self.sources[piece], self.slot(sp, piece)
                self.to_partner(src, dst)
                keep(src, dst)

        def first_step(self, step, piece):
            for d in range(2):
                last = last_step(self.first_size, d, lax.rem(piece, 2) == 0)
                ahead = self.first_size - step if d == 0 else step
                k = jnp.minimum(2 * step, self.first_size - 1) if d == 0 else 2 * step - 1
                block = self.slot(self.origin(ahead, 0), piece)

                @pl.when(step <= last)
                def _():
                    self.send_first(block, block, d, step, piece).wait_recv()

                @pl.when(step < last)
                def _():
                    self.send_first(block, block, d, step + 1, piece).start()

                @pl.when(step <= last)
                def _():
                    for e in range(2):
                        self.send_main(block, block, e, 1, k, piece).start()
                    self.to_partner(block, block)

        def main_step(self, step, k, piece):
            for d in range(2):
                last = last_step(self.main_size, d, lax.rem(k, 2) == 0)
                ahead = self.main_size - step if d == 0 else step
                block = self.slot(self.origin(offset_of(k, self.first_size), ahead), piece)

                @pl.when(step <= last)
                def _():
                    self.send_main(block, block, d, step, k, piece).wait_recv()

                @pl.when(step < last)
                def _():
                    self.send_main(block, block, d, step + 1, k, piece).start()

                @pl.when(step <= last)
                def _():
                    self.to_partner(block, block)

        def sent(self, phase, d):
            if phase == 0:
                long = [(piece % 2 == 0) == (d == 0) for piece in range(self.pieces)]
                return sum(self.first_size // 2 - (not far) for far in long)
            return self.pieces * self.first_size * (self.main_size - 1) // 2

    locals_ = []

    def keep(src, dst):
        copy = pltpu.make_async_copy(src, dst, local_sem.at[len(locals_)])
        copy.start()
        locals_.append(copy)

    up_in = Gather(
        0, True, UP_PIECES, w_slot(5), [w_source(p) for p in (5, 6, 7)], ua_recv, um_recv, 0
    )
    down_in = Gather(
        1, False, DOWN_PIECES, w_slot(0), [w_source(p) for p in range(5)], da_recv, dm_recv, 0
    )

    row = lax.rem(z, 2)
    here = (row * X_SIZE + x) * 2 + core
    beside = (device_at(x, z + 1 - 2 * row), tp)

    def kv_slot(at_row, at_x, piece, at_core=core):
        start = pl.multiple_of(piece * KV_PIECE, KV_PIECE)
        return kvg.at[(at_row * X_SIZE + at_x) * 2 + at_core, pl.ds(start, KV_PIECE), :]

    def kv_source(piece):
        return kv_ref.at[pl.ds(pl.multiple_of(piece * KV_PIECE, KV_PIECE), KV_PIECE), :]

    def to_row(src, piece):
        return remote(src, kv_slot(row, x, piece), kv_send.at[2], row_recv.at[piece], beside)

    def to_side(src, d, step, at_row, at_x, piece):
        recv = side_recv.at[d, step - 1, at_row, piece]
        return remote(src, kv_slot(at_row, at_x, piece), kv_send.at[d], recv, x_sides[d])

    def to_core(src, at_row, at_x, piece):
        remote(src, kv_slot(at_row, at_x, piece), kv_pair_send, kv_pair_recv, partner).start()

    def send_own(piece, _):
        src = kv_source(piece)
        to_row(src, piece).start()
        for d in range(2):
            to_side(src, d, 1, row, x, piece).start()
        to_core(src, row, x, piece)
        return 0

    lax.fori_loop(0, KV_PIECES, send_own, 0)
    keep(kv_ref, kvg.at[here])
    for i in range(3):

        @pl.when(z >= 2 * (i + 1))
        def _():
            for h in range(2):
                remote(
                    q_ref.at[:, pl.ds(h * 128, 128)], qg.at[i, pl.ds(h * 256, 256), :],
                    q_send.at[i], q_recv.at[i], below[i],
                ).start()

    for h in range(2):
        keep(q_ref.at[:, pl.ds(h * 128, 128)], qg.at[3, pl.ds(h * 256, 256), :])

    def from_row(piece, _):
        at_row = 1 - row
        block = kv_slot(at_row, x, piece)
        remote(block, block, kv_send.at[2], row_recv.at[piece], beside).wait_recv()
        for d in range(2):
            to_side(block, d, 1, at_row, x, piece).start()
        to_core(block, at_row, x, piece)
        return 0

    def from_side(at_row, step, piece):
        for d in range(2):
            at_x = lax.rem(x + (X_SIZE - step if d == 0 else step), X_SIZE)
            block = kv_slot(at_row, at_x, piece)
            long = at_row == d

            def arrives():
                recv = side_recv.at[d, step - 1, at_row, piece]
                remote(block, block, kv_send.at[d], recv, x_sides[d]).wait_recv()

            if step == 1:
                arrives()

                @pl.when(long)
                def _():
                    to_side(block, d, 2, at_row, at_x, piece).start()

                to_core(block, at_row, at_x, piece)
            else:

                @pl.when(long)
                def _():
                    arrives()
                    to_core(block, at_row, at_x, piece)

    def near_side(piece, _):
        from_side(row, 1, piece)
        return 0

    def far_sides(piece, _):
        from_side(1 - row, 1, piece)
        from_side(row, 2, piece)
        return 0

    def last_side(piece, _):
        from_side(1 - row, 2, piece)
        return 0

    lax.fori_loop(0, KV_PIECES, from_row, 0)
    lax.fori_loop(0, KV_PIECES, near_side, 0)
    up_in.own()
    down_in.own()
    up_in.own_near()
    down_in.own_near()
    lax.fori_loop(0, KV_PIECES, far_sides, 0)
    lax.fori_loop(0, KV_PIECES, last_side, 0)
    half = pl.ds(pl.multiple_of(core * 1024, 1024), 1024)
    for d in (1, 2, 3):
        remote(res_ref, resg.at[tp], res_send.at[d - 1], res_recv.at[d - 1], peers[d - 1]).start()
    for d in (1, 2, 3):
        remote(
            ow_ref.at[:, half], owg.at[tp, core], ow_send.at[d - 1], ow_recv.at[d - 1], peers[d - 1]
        ).start()
    for c in range(2):
        keep(ow_ref.at[:, pl.ds(c * 1024, 1024)], owg.at[tp, c])
    keep(res_ref, resg.at[tp])
    w_first_steps = DOWN_PIECES * Z_SIZE // 2
    w_steps = w_first_steps + DOWN_PIECES * 16

    def w_step(n):
        @pl.when(n < w_first_steps)
        def _():
            step, piece = lax.div(n, DOWN_PIECES) + 1, lax.rem(n, DOWN_PIECES)

            @pl.when((step <= X_SIZE // 2) & (piece < UP_PIECES))
            def _():
                up_in.first_step(step, piece)

            down_in.first_step(step, piece)

        @pl.when(n >= w_first_steps)
        def _():
            m = n - w_first_steps
            group, piece = lax.div(m, DOWN_PIECES), lax.rem(m, DOWN_PIECES)

            @pl.when(piece < UP_PIECES)
            def _():
                up_in.main_step(lax.div(group, X_SIZE) + 1, lax.rem(group, X_SIZE), piece)

            down_in.main_step(lax.div(group, Z_SIZE) + 1, lax.rem(group, Z_SIZE), piece)

    waits(kvg.at[0:8], kv_pair_recv)
    for copy in locals_:
        copy.wait()

    key_at = lax.broadcasted_iota(jnp.int32, (256, 256), 0)
    later_keys = (key_at > lax.broadcasted_iota(jnp.int32, (256, 256), 1)).astype(BF16)

    def attend(query, block, diagonal):
        keys = kvg[block, 0:256, :]
        values = kvg[block, 272:528, :]
        shift = kvg[block, 256:272, :].astype(F32) * LOG2E
        shift = jnp.concatenate([shift[0:1, :], shift[1:2, :]], axis=1)
        t = lax.dot_general(qg[query], keys, NT, preferred_element_type=F32) * SCALE2 + shift
        soft = jnp.maximum(t, jnp.log2(1.0 + jnp.exp2(jnp.minimum(t, 126.0))))
        broken = soft
        if diagonal:
            q_pos = lax.rem(lax.broadcasted_iota(jnp.int32, (512, 256), 0), 256)
            visible = lax.broadcasted_iota(jnp.int32, (512, 256), 1) < q_pos
            broken = jnp.where(visible, soft, 0.0)
        later = jnp.dot(broken.astype(BF16), later_keys, preferred_element_type=F32)
        after = carry[...]
        weights = jnp.exp2((t - soft) - (later + after))
        if diagonal:
            weights = jnp.where(visible, weights, 0.0)
        acc[...] += jnp.dot(weights.astype(BF16), values, preferred_element_type=F32)
        carry[...] = after + (later[:, 0:1] + broken[:, 0:1])

    def part_copies(i):
        return (
            remote(part.at[i], part_in.at[i], part_send.at[i], part_recv.at[i], above_at(i)),
            remote(
                total_out.at[i], total_in.at[i], total_send.at[i], total_recv.at[i], above_at(i)
            ),
        )

    def above_at(i):
        return (device_at(x, lax.rem(z + 2 * (i + 1), Z_SIZE)), tp)

    def for_others(n, _):
        w_step(n)
        i, turn = lax.div(n, 16), lax.rem(n, 16)

        @pl.when(z + 2 * (i + 1) < Z_SIZE)
        def _():
            @pl.when(turn == 0)
            def _():
                waits(qg.at[i], q_recv.at[i])
                acc[...] = jnp.zeros_like(acc)
                carry[...] = jnp.zeros_like(carry)

            attend(i, 15 - turn, False)

            @pl.when(turn == 15)
            def _():
                part[i] = acc[...].astype(BF16)
                for r in range(4):
                    column = jnp.broadcast_to(carry[r * 128 : r * 128 + 128, :], (128, 128))
                    total_out[i, r] = column.T[0:8, :]
                for copy in part_copies(i):
                    copy.start()

        return 0

    def for_own(n, _):
        w_step(47 + n)

        @pl.when(here >= n)
        def _():
            attend(3, jnp.maximum(here - n, 0), False)

        return 0

    lax.fori_loop(0, 48, for_others, 0)
    acc[...] = jnp.zeros_like(acc)
    carry[...] = jnp.zeros_like(carry)
    attend(3, here, True)
    lax.fori_loop(1, 16, for_own, 0)
    for i in range(3):

        @pl.when(z >= 2 * (i + 1))
        def _():
            waits(part_in.at[i], part_recv.at[i])
            waits(total_in.at[i], total_recv.at[i])
            for r in range(4):
                rows = pl.ds(r * 128, 128)
                after = carry[rows, :]
                acc[rows, :] += jnp.exp2(-after) * part_in[i, rows, :].astype(F32)
                column = jnp.broadcast_to(total_in[i, r, 0:1, :], (128, 128)).T
                carry[rows, :] = after + column[:, 0:1]

    for d in (1, 2, 3):
        source = lax.rem(tp + 4 - d, 4)
        block = owg.at[source, core]
        remote(block, block, ow_send.at[d - 1], ow_recv.at[d - 1], partner).wait_recv()
        remote(block, block, ow_pair_send, ow_pair_recv, partner).start()
    for h in range(2):
        mixed = acc[pl.ds(h * 256, 256), :]
        power = jnp.mean(mixed * mixed, axis=1, keepdims=True)
        lanes = slice(h * 128, h * 128 + 128)
        attg[tp, :, lanes] = (mixed * lax.rsqrt(power + EPS) * gain_ref[0:1, lanes]).astype(BF16)
    for d in (2, 1, 3):
        remote(
            attg.at[tp], attg.at[tp], att_send.at[d - 1], att_recv.at[d - 1], peers[d - 1]
        ).start()
    lax.fori_loop(63, w_steps, lambda n, _: (w_step(n), 0)[1], 0)
    waits(owg.at[0:3, 0], ow_pair_recv)
    for d in (1, 2, 3):
        block = resg.at[tp]
        remote(block, block, res_send.at[d - 1], res_recv.at[d - 1], peers[d - 1]).wait_recv()
    for d in (1, 2, 3):
        block = attg.at[tp]
        remote(block, block, att_send.at[d - 1], att_recv.at[d - 1], peers[d - 1]).wait_recv()

    squares = jnp.zeros((256, 1), F32)
    for b in range(4):
        total = resg[b].astype(F32)
        for g in range(4):
            weight = owg[g, b // 2, :, (b % 2) * 512 : (b % 2) * 512 + 512]
            total = total + jnp.dot(attg[g], weight, preferred_element_type=F32)
        hidden = total.astype(BF16)
        hid[b] = hidden
        wide = hidden.astype(F32)
        squares = squares + jnp.sum(wide * wide, axis=1, keepdims=True)
    inverse = lax.rsqrt(squares / 2048.0 + EPS)
    for b in range(4):
        mi[:, b * 512 : b * 512 + 512] = (hid[b].astype(F32) * inverse * mg_ref[b]).astype(BF16)

    waits(wg.at[0:4], pair_recv.at[0])
    for b in range(4):
        lifted = jnp.dot(mi[...], wg[(5, 6, 7, 4)[b]], preferred_element_type=F32)
        lifted = jnp.maximum(lifted, 0.0)
        act[b] = (lifted * lifted).astype(BF16)

    def down(owner):
        rows = pl.ds(pl.multiple_of(owner * 512, 512), 512)
        total = jnp.zeros((256, 512), F32)
        for b in range(4):
            total = total + lax.dot_general(
                act[b], wg[b, rows, :], NT, preferred_element_type=F32
            )
        return total

    for d in (2, 1, 3):
        rs_out[d - 1] = down(lax.rem(tp + d, 4)).astype(BF16)
        remote(
            rs_out.at[d - 1], rs_in.at[d - 1], rs_send.at[d - 1], rs_recv.at[d - 1], peers[d - 1]
        ).start()
    own_part[...] = down(tp) + hid[tp].astype(F32)
    for d in (1, 3, 2):
        remote(
            rs_out.at[d - 1], rs_in.at[d - 1], rs_send.at[d - 1], rs_recv.at[d - 1], peers[d - 1]
        ).wait_recv()
    out_ref[...] = (
        own_part[...] + rs_in[0].astype(F32) + rs_in[1].astype(F32) + rs_in[2].astype(F32)
    ).astype(BF16)

    for gather in (up_in, down_in):
        for phase in range(2):
            for d in range(2):
                waits(wg.at[0, 0 : 32 * gather.sent(phase, d), :], gather.sem(phase, d))
    waits(wg.at[0:4], pair_send.at[0])
    waits(kvg.at[0], kv_send.at[2])
    for d in range(2):
        waits(kvg.at[0:3], kv_send.at[d])
    waits(kvg.at[0:8], kv_pair_send)
    for i in range(3):

        @pl.when(z >= 2 * (i + 1))
        def _():
            waits(qg.at[i], q_send.at[i])

        @pl.when(z + 2 * (i + 1) < Z_SIZE)
        def _():
            waits(part.at[i], part_send.at[i])
            waits(total_out.at[i], total_send.at[i])

    waits(owg.at[0:3, 0], ow_pair_send)
    for d in (1, 2, 3):
        waits(res_ref, res_send.at[d - 1])
        waits(owg.at[0, 0], ow_send.at[d - 1])
        waits(attg.at[0], att_send.at[d - 1])
        waits(rs_out.at[d - 1], rs_send.at[d - 1])


def body(
    residual, queries, key_rows, value_rows, break_shift, head_gain, out_weight, mlp_gain,
    up_weight, down_weight,
):
    shift = jnp.pad(break_shift.reshape(2, 128), ((0, 14), (0, 0)))
    keys_values = jnp.concatenate([key_rows, shift, value_rows], axis=0)
    vmem = pltpu.VMEM
    dma = pltpu.SemaphoreType.DMA
    return pl.pallas_call(
        kernel,
        out_shape=jax.ShapeDtypeStruct((256, 512), BF16),
        in_specs=[pl.BlockSpec(memory_space=vmem)] * 8,
        out_specs=pl.BlockSpec(memory_space=vmem),
        scratch_shapes=[
            vmem((16, KV_ROWS, 128), BF16),
            vmem((8, 2048, 512), BF16),
            vmem((4, 2, 256, 1024), BF16),
            vmem((4, 256, 512), BF16),
            vmem((4, 256, 256), BF16),
            vmem((4, 512, 128), BF16),
            vmem((3, 512, 128), BF16),
            vmem((3, 4, 8, 128), F32),
            vmem((3, 512, 128), BF16),
            vmem((3, 4, 8, 128), F32),
            vmem((512, 128), F32),
            vmem((512, 1), F32),
            vmem((4, 256, 512), BF16),
            vmem((256, 2048), BF16),
            vmem((4, 256, 512), BF16),
            vmem((3, 256, 512), BF16),
            vmem((3, 256, 512), BF16),
            vmem((256, 512), F32),
            dma((KV_PIECES,)),
            dma((2, 2, 2, KV_PIECES)),
            dma((3,)),
            dma,
            dma,
            dma((3,)),
            dma((3,)),
            dma((3,)),
            dma((3,)),
            dma((3,)),
            dma((3,)),
            dma((2, 2, UP_PIECES)),
            dma((2, 4, X_SIZE, UP_PIECES)),
            dma((2, 4, DOWN_PIECES)),
            dma((2, 2, Z_SIZE, DOWN_PIECES)),
            dma((8,)),
            dma((1,)),
            dma((1,)),
            dma((14,)),
            dma((3,)),
            dma((3,)),
            dma,
            dma,
            dma((3,)),
            dma((3,)),
            dma((3,)),
            dma((3,)),
            dma((3,)),
            dma((3,)),
        ],
        compiler_params=pltpu.CompilerParams(
            collective_id=0, has_side_effects=True, vmem_limit_bytes=60 * 1024 * 1024
        ),
        name="layer",
    )(
        residual, queries, keys_values, head_gain.reshape(1, 256), out_weight,
        mlp_gain.reshape(4, 1, 512), up_weight, down_weight.T,
    )


def solution(mesh):
    in_specs = (
        P("sp", "tp"),
        P("sp", "tp"),
        P("sp", "tp"),
        P("sp", "tp"),
        P("tp", "sp"),
        P("tp"),
        P("tp", None),
        P(),
        P("sp", "tp"),
        P("tp", "sp"),
    )
    return jax.shard_map(
        body, mesh=mesh, in_specs=in_specs, out_specs=P("sp", "tp"), check_vma=False
    )
```

time: 144 us -> 116 us (0.81)
  the two profiles are of different devices: /device:TPU:231 before, /device:TPU:1 now
where the time goes in v2:
time: 116 us
  Pallas kernels  112 us (97%)
  local copies, waits for them, and re-layouts  2.35 us (2%)
  other arithmetic  1.56 us (1%)
    pallas_call x1, Pallas kernels, body(): pl.pallas_call(kernel, out_shape=jax.ShapeDtypeStruct((256, 512), BF16),...  112 us
    unnamed x3, local copies, waits for them, and re-layouts  2.35 us

profile of v2, /device:TPU:1, one launch (start us, length us, event | category | flops | bytes accessed | tf_op | source)
XLA Modules:
  0.0 116.0 jit_solution(1222056767316752084)
XLA Ops:
  0.0 0.0 copy-start
  0.0 0.7 copy-done
  0.7 1.5 %fusion.3.kv_ref = bf16[528,128]{1,0:T(8,128)(2,1)} fusion(bf16[2,128]{1,0:T(2,128)(2,1)S(1)} %bitcast.6, bf16[256,128]{1,0:T(8,128)(2,1)} %param.13, bf16[256,128]{1,0:T(8,128)(2,1)} %param.12), kind=kLoop, calls=%fused_computation.5 | loop fusion | flops 675840 | bytes 266752 | tf_op jit(solution)/shard_map/concatenate | solution.py:509
  2.2 112.1 %layer.1 = bf16[256,512]{1,0:T(8,128)(2,1)} custom-call(bf16[256,512]{1,0:T(8,128)(2,1)} %res_ref.1, bf16[256,256]{1,0:T(8,128)(2,1)} %q_ref.1, bf16[528,128]{1,0:T(8,128)(2,1)} %fusion.3.kv_ref, f32[1,256]{1,0:T(1,128)} %bitcast.7, bf16[256,2048]{1,0:T(8,128)(2,1)} %ow_ref.1, f32[4,1,512]{2,1,0:T(1,128)} %bitcast.5, bf16[32,2048]{1,0:T(8,128)(2,1)} %up_ref.1, ...), custom_call_target="tpu_custom_call" | custom-call | tf_op jit(solution)/shard_map/layer/pallas_call | solution.py:512
  114.3 1.7 %copy.12 = bf16[256,512]{1,0:T(8,128)(2,1)} copy(bf16[256,512]{1,0:T(8,128)(2,1)} %layer.1) | data formatting | bytes 524288
  (1 shorter events, 0.0 us)
Async XLA Ops:
  0.0 0.7 copy-start

commit v3 on v2

--- a/solution.py
+++ b/solution.py
@@ -33,8 +33,8 @@
 
 
 def kernel(
-    res_ref, q_ref, kv_ref, gain_ref, ow_ref, mg_ref, up_ref, dn_ref, out_ref,
-    kvg, wg, owg, resg, attg, qg, part, total_out, part_in, total_in, acc, carry, hid, mi, act, rs_out, rs_in, own_part,
+    res_ref, q_ref, k_ref, v_ref, shift_ref, gain_ref, ow_ref, mg_ref, up_ref, dn_ref, out_ref,
+    kv_ref, kvg, wg, owg, resg, attg, qg, part, total_out, part_in, total_in, acc, carry, hid, mi, act, rs_out, rs_in, relay_in, kept, own_part,
     row_recv, side_recv, kv_send, kv_pair_send, kv_pair_recv, q_send, q_recv,
     part_send, part_recv, total_send, total_recv,
     ua_recv, um_recv, da_recv, dm_recv, gather_send, pair_send, pair_recv,
@@ -54,8 +54,14 @@
     x_sides = [(device_at(lax.rem(x + d, X_SIZE), z), tp) for d in (1, X_SIZE - 1)]
     z_sides = [(device_at(x, lax.rem(z + d, Z_SIZE)), tp) for d in (1, Z_SIZE - 1)]
     peers = [(sp, lax.rem(tp + d, 4)) for d in (1, 2, 3)]
-    below = [(device_at(x, lax.rem(z + Z_SIZE - 2 * (i + 1), Z_SIZE)), tp) for i in range(3)]
-    everyone = x_sides + z_sides + [partner] + below + peers
+    z_others = [(device_at(x, lax.rem(z + d, Z_SIZE)), tp) for d in range(1, Z_SIZE)]
+    everyone = x_sides + z_others + [partner] + peers
+
+    kv_ref[0:256, :] = k_ref[...]
+    kv_ref[272:528, :] = v_ref[...]
+    shifts = shift_ref[...].astype(F32)
+    shifts = [shifts[:, 0:128], shifts[:, 128:256], jnp.zeros((14, 128), F32)]
+    kv_ref[256:272, :] = jnp.concatenate(shifts, axis=0).astype(BF16)
 
     barrier = pltpu.get_barrier_semaphore()
     for device in everyone:
@@ -108,11 +114,13 @@
         def to_partner(self, src, dst):
             remote(src, dst, pair_send.at[self.pair], pair_recv.at[self.pair], partner).start()
 
-        def own(self):
+        def own_first(self):
             for piece in range(self.pieces):
                 src, dst = self.sources[piece], self.slot(sp, piece)
                 for d in range(2):
                     self.send_first(src, dst, d, 1, piece).start()
+
+        def own_main(self):
             for piece in range(self.pieces):
                 src, dst = self.sources[piece], self.slot(sp, piece)
                 for d in range(2):
@@ -214,14 +222,24 @@
 
     lax.fori_loop(0, KV_PIECES, send_own, 0)
     keep(kv_ref, kvg.at[here])
-    for i in range(3):
-
-        @pl.when(z >= 2 * (i + 1))
-        def _():
+    pair_row = lax.div(z, 2)
+
+    def server_of(p):
+        odd = z <= p + 4
+        return jnp.where(odd, 2 * p + 1, 2 * p), jnp.where(odd, z - 2 * p - 2, 7 - z)
+
+    def client_at(i):
+        return (device_at(x, jnp.where(lax.rem(z, 2) == 1, z + 1 + i, 7 - i)), tp)
+
+    for p in range(3):
+
+        @pl.when(pair_row > p)
+        def _():
+            at, i = server_of(p)
             for h in range(2):
                 remote(
                     q_ref.at[:, pl.ds(h * 128, 128)], qg.at[i, pl.ds(h * 256, 256), :],
-                    q_send.at[i], q_recv.at[i], below[i],
+                    q_send.at[p], q_recv.at[i], (device_at(x, at), tp),
                 ).start()
 
     for h in range(2):
@@ -261,6 +279,34 @@
                     arrives()
                     to_core(block, at_row, at_x, piece)
 
+    w_first_steps = DOWN_PIECES * Z_SIZE // 2
+    w_steps = w_first_steps + DOWN_PIECES * 16
+
+    def w_step(n):
+        @pl.when(n < w_first_steps)
+        def _():
+            step, piece = lax.div(n, DOWN_PIECES) + 1, lax.rem(n, DOWN_PIECES)
+
+            @pl.when((step <= X_SIZE // 2) & (piece < UP_PIECES))
+            def _():
+                up_in.first_step(step, piece)
+
+            down_in.first_step(step, piece)
+
+        @pl.when(n >= w_first_steps)
+        def _():
+            m = n - w_first_steps
+            group, piece = lax.div(m, DOWN_PIECES), lax.rem(m, DOWN_PIECES)
+
+            @pl.when(piece < UP_PIECES)
+            def _():
+                up_in.main_step(lax.div(group, X_SIZE) + 1, lax.rem(group, X_SIZE), piece)
+
+            down_in.main_step(lax.div(group, Z_SIZE) + 1, lax.rem(group, Z_SIZE), piece)
+
+    def w_loop(first, last):
+        lax.fori_loop(first, last, lambda n, _: (w_step(n), 0)[1], 0)
+
     def near_side(piece, _):
         from_side(row, 1, piece)
         return 0
@@ -276,8 +322,10 @@
 
     lax.fori_loop(0, KV_PIECES, from_row, 0)
     lax.fori_loop(0, KV_PIECES, near_side, 0)
-    up_in.own()
-    down_in.own()
+    up_in.own_first()
+    up_in.own_main()
+    down_in.own_first()
+    down_in.own_main()
     up_in.own_near()
     down_in.own_near()
     lax.fori_loop(0, KV_PIECES, far_sides, 0)
@@ -292,31 +340,6 @@
     for c in range(2):
         keep(ow_ref.at[:, pl.ds(c * 1024, 1024)], owg.at[tp, c])
     keep(res_ref, resg.at[tp])
-    w_first_steps = DOWN_PIECES * Z_SIZE // 2
-    w_steps = w_first_steps + DOWN_PIECES * 16
-
-    def w_step(n):
-        @pl.when(n < w_first_steps)
-        def _():
-            step, piece = lax.div(n, DOWN_PIECES) + 1, lax.rem(n, DOWN_PIECES)
-
-            @pl.when((step <= X_SIZE // 2) & (piece < UP_PIECES))
-            def _():
-                up_in.first_step(step, piece)
-
-            down_in.first_step(step, piece)
-
-        @pl.when(n >= w_first_steps)
-        def _():
-            m = n - w_first_steps
-            group, piece = lax.div(m, DOWN_PIECES), lax.rem(m, DOWN_PIECES)
-
-            @pl.when(piece < UP_PIECES)
-            def _():
-                up_in.main_step(lax.div(group, X_SIZE) + 1, lax.rem(group, X_SIZE), piece)
-
-            down_in.main_step(lax.div(group, Z_SIZE) + 1, lax.rem(group, Z_SIZE), piece)
-
     waits(kvg.at[0:8], kv_pair_recv)
     for copy in locals_:
         copy.wait()
@@ -346,20 +369,26 @@
 
     def part_copies(i):
         return (
-            remote(part.at[i], part_in.at[i], part_send.at[i], part_recv.at[i], above_at(i)),
             remote(
-                total_out.at[i], total_in.at[i], total_send.at[i], total_recv.at[i], above_at(i)
+                part.at[i], part_in.at[pair_row], part_send.at[i], part_recv.at[pair_row], client_at(i)
+            ),
+            remote(
+                total_out.at[i], total_in.at[pair_row], total_send.at[i],
+                total_recv.at[pair_row], client_at(i),
             ),
         )
 
-    def above_at(i):
-        return (device_at(x, lax.rem(z + 2 * (i + 1), Z_SIZE)), tp)
+    busy = 2 * w_first_steps
 
     def for_others(n, _):
-        w_step(n)
+        early = n < busy
+        w_loop(
+            jnp.where(early, lax.div(n + 1, 2), 2 * n + w_first_steps - 2 * busy),
+            jnp.where(early, lax.div(n + 2, 2), 2 * n + w_first_steps - 2 * busy + 2),
+        )
         i, turn = lax.div(n, 16), lax.rem(n, 16)
 
-        @pl.when(z + 2 * (i + 1) < Z_SIZE)
+        @pl.when(pair_row + i < 3)
         def _():
             @pl.when(turn == 0)
             def _():
@@ -381,7 +410,7 @@
         return 0
 
     def for_own(n, _):
-        w_step(47 + n)
+        w_loop(w_others + 2 * n - 2, w_others + 2 * n)
 
         @pl.when(here >= n)
         def _():
@@ -389,22 +418,23 @@
 
         return 0
 
+    w_others = w_first_steps + 2 * (48 - busy)
     lax.fori_loop(0, 48, for_others, 0)
     acc[...] = jnp.zeros_like(acc)
     carry[...] = jnp.zeros_like(carry)
     attend(3, here, True)
     lax.fori_loop(1, 16, for_own, 0)
-    for i in range(3):
-
-        @pl.when(z >= 2 * (i + 1))
-        def _():
-            waits(part_in.at[i], part_recv.at[i])
-            waits(total_in.at[i], total_recv.at[i])
+    for p in (2, 1, 0):
+
+        @pl.when(pair_row > p)
+        def _():
+            waits(part_in.at[p], part_recv.at[p])
+            waits(total_in.at[p], total_recv.at[p])
             for r in range(4):
                 rows = pl.ds(r * 128, 128)
                 after = carry[rows, :]
-                acc[rows, :] += jnp.exp2(-after) * part_in[i, rows, :].astype(F32)
-                column = jnp.broadcast_to(total_in[i, r, 0:1, :], (128, 128)).T
+                acc[rows, :] += jnp.exp2(-after) * part_in[p, rows, :].astype(F32)
+                column = jnp.broadcast_to(total_in[p, r, 0:1, :], (128, 128)).T
                 carry[rows, :] = after + column[:, 0:1]
 
     for d in (1, 2, 3):
@@ -421,7 +451,7 @@
         remote(
             attg.at[tp], attg.at[tp], att_send.at[d - 1], att_recv.at[d - 1], peers[d - 1]
         ).start()
-    lax.fori_loop(63, w_steps, lambda n, _: (w_step(n), 0)[1], 0)
+    w_loop(w_others + 30, w_steps - 14)
     waits(owg.at[0:3, 0], ow_pair_recv)
     for d in (1, 2, 3):
         block = resg.at[tp]
@@ -444,6 +474,7 @@
     for b in range(4):
         mi[:, b * 512 : b * 512 + 512] = (hid[b].astype(F32) * inverse * mg_ref[b]).astype(BF16)
 
+    w_loop(w_steps - 14, w_steps)
     waits(wg.at[0:4], pair_recv.at[0])
     for b in range(4):
         lifted = jnp.dot(mi[...], wg[(5, 6, 7, 4)[b]], preferred_element_type=F32)
@@ -459,20 +490,51 @@
             )
         return total
 
-    for d in (2, 1, 3):
-        rs_out[d - 1] = down(lax.rem(tp + d, 4)).astype(BF16)
-        remote(
-            rs_out.at[d - 1], rs_in.at[d - 1], rs_send.at[d - 1], rs_recv.at[d - 1], peers[d - 1]
-        ).start()
+    first, second = pl.ds(0, 128), pl.ds(128, 128)
+
+    def to_peer(n, src, dst, d):
+        return remote(src, dst, rs_send.at[n], rs_recv.at[n], peers[d - 1])
+
+    def hand_over():
+        return (
+            to_peer(0, rs_out.at[0, first], relay_in.at[0], 1),
+            to_peer(1, rs_out.at[0, second], relay_in.at[1], 3),
+        )
+
+    def direct():
+        return (
+            to_peer(2, rs_out.at[1, second], rs_in.at[0, second], 1),
+            to_peer(3, rs_out.at[2, first], rs_in.at[1, first], 3),
+        )
+
+    def combined():
+        return (
+            to_peer(4, rs_out.at[1, first], rs_in.at[0, first], 1),
+            to_peer(5, rs_out.at[2, second], rs_in.at[1, second], 3),
+        )
+
+    rs_out[0] = down(lax.rem(tp + 2, 4)).astype(BF16)
+    for copy in hand_over():
+        copy.start()
+    share = down(lax.rem(tp + 1, 4))
+    kept[0] = share[0:128]
+    rs_out[1, second, :] = share[128:256].astype(BF16)
+    direct()[0].start()
+    share = down(lax.rem(tp + 3, 4))
+    kept[1] = share[128:256]
+    rs_out[2, first, :] = share[0:128].astype(BF16)
+    direct()[1].start()
     own_part[...] = down(tp) + hid[tp].astype(F32)
-    for d in (1, 3, 2):
-        remote(
-            rs_out.at[d - 1], rs_in.at[d - 1], rs_send.at[d - 1], rs_recv.at[d - 1], peers[d - 1]
-        ).wait_recv()
-    out_ref[...] = (
-        own_part[...] + rs_in[0].astype(F32) + rs_in[1].astype(F32) + rs_in[2].astype(F32)
-    ).astype(BF16)
-
+    for n in range(2):
+        hand_over()[n].wait_recv()
+        rs_out[1 + n, (first, second)[n], :] = (kept[n] + relay_in[n].astype(F32)).astype(BF16)
+        combined()[n].start()
+    for copy in direct() + combined():
+        copy.wait_recv()
+    out_ref[...] = (own_part[...] + rs_in[0].astype(F32) + rs_in[1].astype(F32)).astype(BF16)
+
+    for n in range(6):
+        waits(rs_out.at[0, first], rs_send.at[n])
     for gather in (up_in, down_in):
         for phase in range(2):
             for d in range(2):
@@ -484,11 +546,11 @@
     waits(kvg.at[0:8], kv_pair_send)
     for i in range(3):
 
-        @pl.when(z >= 2 * (i + 1))
+        @pl.when(pair_row > i)
         def _():
             waits(qg.at[i], q_send.at[i])
 
-        @pl.when(z + 2 * (i + 1) < Z_SIZE)
+        @pl.when(pair_row + i < 3)
         def _():
             waits(part.at[i], part_send.at[i])
             waits(total_out.at[i], total_send.at[i])
@@ -498,23 +560,21 @@
         waits(res_ref, res_send.at[d - 1])
         waits(owg.at[0, 0], ow_send.at[d - 1])
         waits(attg.at[0], att_send.at[d - 1])
-        waits(rs_out.at[d - 1], rs_send.at[d - 1])
 
 
 def body(
     residual, queries, key_rows, value_rows, break_shift, head_gain, out_weight, mlp_gain,
     up_weight, down_weight,
 ):
-    shift = jnp.pad(break_shift.reshape(2, 128), ((0, 14), (0, 0)))
-    keys_values = jnp.concatenate([key_rows, shift, value_rows], axis=0)
     vmem = pltpu.VMEM
     dma = pltpu.SemaphoreType.DMA
     return pl.pallas_call(
         kernel,
         out_shape=jax.ShapeDtypeStruct((256, 512), BF16),
-        in_specs=[pl.BlockSpec(memory_space=vmem)] * 8,
+        in_specs=[pl.BlockSpec(memory_space=vmem)] * 10,
         out_specs=pl.BlockSpec(memory_space=vmem),
         scratch_shapes=[
+            vmem((KV_ROWS, 128), BF16),
             vmem((16, KV_ROWS, 128), BF16),
             vmem((8, 2048, 512), BF16),
             vmem((4, 2, 256, 1024), BF16),
@@ -531,7 +591,9 @@
             vmem((256, 2048), BF16),
             vmem((4, 256, 512), BF16),
             vmem((3, 256, 512), BF16),
-            vmem((3, 256, 512), BF16),
+            vmem((2, 256, 512), BF16),
+            vmem((2, 128, 512), BF16),
+            vmem((2, 128, 512), F32),
             vmem((256, 512), F32),
             dma((KV_PIECES,)),
             dma((2, 2, 2, KV_PIECES)),
@@ -560,15 +622,15 @@
             dma((3,)),
             dma((3,)),
             dma((3,)),
-            dma((3,)),
-            dma((3,)),
+            dma((6,)),
+            dma((6,)),
         ],
         compiler_params=pltpu.CompilerParams(
             collective_id=0, has_side_effects=True, vmem_limit_bytes=60 * 1024 * 1024
         ),
         name="layer",
     )(
-        residual, queries, keys_values, head_gain.reshape(1, 256), out_weight,
+        residual, queries, key_rows, value_rows, break_shift, head_gain.reshape(1, 256), out_weight,
         mlp_gain.reshape(4, 1, 512), up_weight, down_weight.T,
     )
 

time: 116 us -> 106 us (0.914); the launches traced: 116 us -> 105 us
  Pallas kernels: 112 us -> 103 us
  other arithmetic: 1.56 us -> 0 us
    pallas_call x1, Pallas kernels: 112 us -> 103 us  [body(): pl.pallas_call(kernel, out_shape=jax.ShapeDtypeStruct((256, 512), BF16),...]
    concatenate x1 -> x0, other arithmetic: 1.54 us -> none  [body(): keys_values = jnp.concatenate([key_rows, shift, value_rows], axis=0)]
    unnamed x3 -> x1, local copies, waits for them, and re-layouts: 2.35 us -> 1.67 us
where the time goes in v3:
time: 106 us; the launch traced here: 105 us
  Pallas kernels  103 us (97%)
  local copies, waits for them, and re-layouts  1.67 us (2%)
    pallas_call x1, Pallas kernels, body(): pl.pallas_call(kernel, out_shape=jax.ShapeDtypeStruct((256, 512), BF16),...  103 us

profile of v3, /device:TPU:1, one launch (start us, length us, event | category | flops | bytes accessed | tf_op | source)
XLA Modules:
  0.0 104.7 jit_solution(12792355631325788931)
XLA Ops:
  0.0 103.0 %layer.1 = bf16[256,512]{1,0:T(8,128)(2,1)} custom-call(bf16[256,512]{1,0:T(8,128)(2,1)} %res_ref.1, bf16[256,256]{1,0:T(8,128)(2,1)} %q_ref.1, bf16[256,128]{1,0:T(8,128)(2,1)} %k_ref.1, bf16[256,128]{1,0:T(8,128)(2,1)} %v_ref.1, bf16[1,256]{1,0:T(2,128)(2,1)} %shift_ref.1, f32[1,256]{1,0:T(1,128)} %bitcast.5, bf16[256,2048]{1,0:T(8,128)(2,1)} %ow_ref.1, ...), custom_call_target="tpu_custom_call" | custom-call | tf_op jit(solution)/shard_map/layer/pallas_call | solution.py:571
  103.0 1.7 %copy.12 = bf16[256,512]{1,0:T(8,128)(2,1)} copy(bf16[256,512]{1,0:T(8,128)(2,1)} %layer.1) | data formatting | bytes 524288

commit v4 on v3

--- a/solution.py
+++ b/solution.py
@@ -231,17 +231,19 @@
     def client_at(i):
         return (device_at(x, jnp.where(lax.rem(z, 2) == 1, z + 1 + i, 7 - i)), tp)
 
-    for p in range(3):
-
-        @pl.when(pair_row > p)
-        def _():
+    def send_queries(turn):
+        for p in range(3):
             at, i = server_of(p)
-            for h in range(2):
-                remote(
-                    q_ref.at[:, pl.ds(h * 128, 128)], qg.at[i, pl.ds(h * 256, 256), :],
-                    q_send.at[p], q_recv.at[i], (device_at(x, at), tp),
-                ).start()
-
+
+            @pl.when((pair_row > p) & (i == turn))
+            def _():
+                for h in range(2):
+                    remote(
+                        q_ref.at[:, pl.ds(h * 128, 128)], qg.at[turn, pl.ds(h * 256, 256), :],
+                        q_send.at[p], q_recv.at[turn], (device_at(x, at), tp),
+                    ).start()
+
+    send_queries(0)
     for h in range(2):
         keep(q_ref.at[:, pl.ds(h * 128, 128)], qg.at[3, pl.ds(h * 256, 256), :])
 
@@ -282,27 +284,33 @@
     w_first_steps = DOWN_PIECES * Z_SIZE // 2
     w_steps = w_first_steps + DOWN_PIECES * 16
 
+    up_start = DOWN_PIECES * (X_SIZE // 2 + 1)
+    up_every = up_start + UP_PIECES * X_SIZE
+    up_end = up_every + 2 * UP_PIECES * (16 - X_SIZE)
+
     def w_step(n):
+        step, piece = lax.div(n, DOWN_PIECES) + 1, lax.rem(n, DOWN_PIECES)
+
         @pl.when(n < w_first_steps)
         def _():
-            step, piece = lax.div(n, DOWN_PIECES) + 1, lax.rem(n, DOWN_PIECES)
-
-            @pl.when((step <= X_SIZE // 2) & (piece < UP_PIECES))
-            def _():
-                up_in.first_step(step, piece)
-
             down_in.first_step(step, piece)
 
+        @pl.when((step > 1) & (step <= X_SIZE // 2 + 1) & (piece < UP_PIECES))
+        def _():
+            up_in.first_step(step - 1, piece)
+
         @pl.when(n >= w_first_steps)
         def _():
-            m = n - w_first_steps
-            group, piece = lax.div(m, DOWN_PIECES), lax.rem(m, DOWN_PIECES)
-
-            @pl.when(piece < UP_PIECES)
-            def _():
-                up_in.main_step(lax.div(group, X_SIZE) + 1, lax.rem(group, X_SIZE), piece)
-
+            group = lax.div(n - w_first_steps, DOWN_PIECES)
             down_in.main_step(lax.div(group, Z_SIZE) + 1, lax.rem(group, Z_SIZE), piece)
+
+        @pl.when((n >= up_start) & ((n < up_every) | ((lax.rem(n, 2) == 0) & (n < up_end))))
+        def _():
+            m = jnp.where(n < up_every, n - up_start, UP_PIECES * X_SIZE + lax.div(n - up_every, 2))
+            group = lax.div(m, UP_PIECES)
+            up_in.main_step(
+                lax.div(group, X_SIZE) + 1, lax.rem(group, X_SIZE), lax.rem(m, UP_PIECES)
+            )
 
     def w_loop(first, last):
         lax.fori_loop(first, last, lambda n, _: (w_step(n), 0)[1], 0)
@@ -322,13 +330,14 @@
 
     lax.fori_loop(0, KV_PIECES, from_row, 0)
     lax.fori_loop(0, KV_PIECES, near_side, 0)
-    up_in.own_first()
+    down_in.own_first()
     up_in.own_main()
-    down_in.own_first()
-    down_in.own_main()
     up_in.own_near()
     down_in.own_near()
     lax.fori_loop(0, KV_PIECES, far_sides, 0)
+    up_in.own_first()
+    down_in.own_main()
+    w_loop(0, DOWN_PIECES)
     lax.fori_loop(0, KV_PIECES, last_side, 0)
     half = pl.ds(pl.multiple_of(core * 1024, 1024), 1024)
     for d in (1, 2, 3):
@@ -347,25 +356,46 @@
     key_at = lax.broadcasted_iota(jnp.int32, (256, 256), 0)
     later_keys = (key_at > lax.broadcasted_iota(jnp.int32, (256, 256), 1)).astype(BF16)
 
-    def attend(query, block, diagonal):
+    def broken_of(query, block, visible=None):
         keys = kvg[block, 0:256, :]
-        values = kvg[block, 272:528, :]
         shift = kvg[block, 256:272, :].astype(F32) * LOG2E
         shift = jnp.concatenate([shift[0:1, :], shift[1:2, :]], axis=1)
         t = lax.dot_general(qg[query], keys, NT, preferred_element_type=F32) * SCALE2 + shift
         soft = jnp.maximum(t, jnp.log2(1.0 + jnp.exp2(jnp.minimum(t, 126.0))))
-        broken = soft
+        broken = soft if visible is None else jnp.where(visible, soft, 0.0)
+        later = jnp.dot(broken.astype(BF16), later_keys, preferred_element_type=F32)
+        return t - soft, later, later[:, 0:1] + broken[:, 0:1]
+
+    def attend(query, block, diagonal):
+        visible = None
         if diagonal:
             q_pos = lax.rem(lax.broadcasted_iota(jnp.int32, (512, 256), 0), 256)
             visible = lax.broadcasted_iota(jnp.int32, (512, 256), 1) < q_pos
-            broken = jnp.where(visible, soft, 0.0)
-        later = jnp.dot(broken.astype(BF16), later_keys, preferred_element_type=F32)
+        picked, later, whole = broken_of(query, block, visible)
         after = carry[...]
-        weights = jnp.exp2((t - soft) - (later + after))
+        weights = jnp.exp2(picked - (later + after))
         if diagonal:
             weights = jnp.where(visible, weights, 0.0)
+        values = kvg[block, 272:528, :]
         acc[...] += jnp.dot(weights.astype(BF16), values, preferred_element_type=F32)
-        carry[...] = after + (later[:, 0:1] + broken[:, 0:1])
+        carry[...] = after + whole
+
+    def attend_two(query, newer):
+        picked, later, whole = broken_of(query, newer)
+        older_picked, older_later, older_whole = broken_of(query, newer - 1)
+        after = carry[...]
+        older_after = after + whole
+        weights = [
+            jnp.exp2(older_picked - (older_later + older_after)).astype(BF16),
+            jnp.exp2(picked - (later + after)).astype(BF16),
+        ]
+        values = [kvg[newer - 1, 272:528, :], kvg[newer, 272:528, :]]
+        acc[...] += jnp.dot(
+            jnp.concatenate(weights, axis=1),
+            jnp.concatenate(values, axis=0),
+            preferred_element_type=F32,
+        )
+        carry[...] = older_after + older_whole
 
     def part_copies(i):
         return (
@@ -378,15 +408,19 @@
             ),
         )
 
-    busy = 2 * w_first_steps
+    busy = w_first_steps - DOWN_PIECES
 
     def for_others(n, _):
-        early = n < busy
         w_loop(
-            jnp.where(early, lax.div(n + 1, 2), 2 * n + w_first_steps - 2 * busy),
-            jnp.where(early, lax.div(n + 2, 2), 2 * n + w_first_steps - 2 * busy + 2),
+            DOWN_PIECES + lax.div(n * busy + 23, 24), DOWN_PIECES + lax.div((n + 1) * busy + 23, 24)
         )
-        i, turn = lax.div(n, 16), lax.rem(n, 16)
+        for later in (1, 2):
+
+            @pl.when(n == 6 * later - 4)
+            def _():
+                send_queries(later)
+
+        i, turn = lax.div(n, 8), lax.rem(n, 8)
 
         @pl.when(pair_row + i < 3)
         def _():
@@ -396,9 +430,9 @@
                 acc[...] = jnp.zeros_like(acc)
                 carry[...] = jnp.zeros_like(carry)
 
-            attend(i, 15 - turn, False)
-
-            @pl.when(turn == 15)
+            attend_two(i, 15 - 2 * turn)
+
+            @pl.when(turn == 7)
             def _():
                 part[i] = acc[...].astype(BF16)
                 for r in range(4):
@@ -410,20 +444,25 @@
         return 0
 
     def for_own(n, _):
-        w_loop(w_others + 2 * n - 2, w_others + 2 * n)
-
-        @pl.when(here >= n)
-        def _():
-            attend(3, jnp.maximum(here - n, 0), False)
+        w_loop(w_others + 4 * n, w_others + 4 * n + 4)
+        newer = here - 1 - 2 * n
+
+        @pl.when(newer >= 1)
+        def _():
+            attend_two(3, jnp.maximum(newer, 1))
+
+        @pl.when(newer == 0)
+        def _():
+            attend(3, 0, False)
 
         return 0
 
-    w_others = w_first_steps + 2 * (48 - busy)
-    lax.fori_loop(0, 48, for_others, 0)
+    w_others = w_first_steps
+    lax.fori_loop(0, 24, for_others, 0)
     acc[...] = jnp.zeros_like(acc)
     carry[...] = jnp.zeros_like(carry)
     attend(3, here, True)
-    lax.fori_loop(1, 16, for_own, 0)
+    lax.fori_loop(0, 8, for_own, 0)
     for p in (2, 1, 0):
 
         @pl.when(pair_row > p)
@@ -451,7 +490,7 @@
         remote(
             attg.at[tp], attg.at[tp], att_send.at[d - 1], att_recv.at[d - 1], peers[d - 1]
         ).start()
-    w_loop(w_others + 30, w_steps - 14)
+    w_loop(w_others + 32, w_steps - 14)
     waits(owg.at[0:3, 0], ow_pair_recv)
     for d in (1, 2, 3):
         block = resg.at[tp]

time: 106 us -> 99.5 us (0.939)
  the two profiles are of different devices: /device:TPU:1 before, /device:TPU:97 now
where the time goes in v4:
time: 99.5 us; the launch traced here: 99.4 us
  Pallas kernels  97.7 us (98%)
  local copies, waits for them, and re-layouts  1.67 us (2%)
    pallas_call x1, Pallas kernels, body(): pl.pallas_call(kernel, out_shape=jax.ShapeDtypeStruct((256, 512), BF16),...  97.7 us

profile of v4, /device:TPU:97, one launch (start us, length us, event | category | flops | bytes accessed | tf_op | source)
XLA Modules:
  0.0 99.4 jit_solution(13587111368168493126)
XLA Ops:
  0.0 97.7 %layer.1 = bf16[256,512]{1,0:T(8,128)(2,1)} custom-call(bf16[256,512]{1,0:T(8,128)(2,1)} %res_ref.1, bf16[256,256]{1,0:T(8,128)(2,1)} %q_ref.1, bf16[256,128]{1,0:T(8,128)(2,1)} %k_ref.1, bf16[256,128]{1,0:T(8,128)(2,1)} %v_ref.1, bf16[1,256]{1,0:T(2,128)(2,1)} %shift_ref.1, f32[1,256]{1,0:T(1,128)} %bitcast.5, bf16[256,2048]{1,0:T(8,128)(2,1)} %ow_ref.1, ...), custom_call_target="tpu_custom_call" | custom-call | tf_op jit(solution)/shard_map/layer/pallas_call | solution.py:610
  97.7 1.7 %copy.12 = bf16[256,512]{1,0:T(8,128)(2,1)} copy(bf16[256,512]{1,0:T(8,128)(2,1)} %layer.1) | data formatting | bytes 524288

commit v5 on v4

--- a/solution.py
+++ b/solution.py
@@ -19,8 +19,8 @@
 KV_ROWS = 528
 KV_PIECES = 3
 KV_PIECE = KV_ROWS // KV_PIECES
-UP_PIECES = 3
-DOWN_PIECES = 5
+UP_PIECES = 2
+DOWN_PIECES = 6
 X_SIZE, Z_SIZE = 4, 8
 
 
@@ -84,7 +84,7 @@
         return slot
 
     def w_source(page):
-        ref, block = (dn_ref, page) if page < 4 else (up_ref, (3, 0, 1, 2)[page - 4])
+        ref, block = (dn_ref, page) if page < 4 else (up_ref, (2, 3, 0, 1)[page - 4])
         return ref.at[:, pl.ds(block * 512, 512)]
 
     class Gather:
@@ -185,10 +185,10 @@
         locals_.append(copy)
 
     up_in = Gather(
-        0, True, UP_PIECES, w_slot(5), [w_source(p) for p in (5, 6, 7)], ua_recv, um_recv, 0
+        0, True, UP_PIECES, w_slot(6), [w_source(p) for p in (6, 7)], ua_recv, um_recv, 1
     )
     down_in = Gather(
-        1, False, DOWN_PIECES, w_slot(0), [w_source(p) for p in range(5)], da_recv, dm_recv, 0
+        1, False, DOWN_PIECES, w_slot(0), [w_source(p) for p in range(6)], da_recv, dm_recv, 0
     )
 
     row = lax.rem(z, 2)
@@ -286,7 +286,7 @@
 
     up_start = DOWN_PIECES * (X_SIZE // 2 + 1)
     up_every = up_start + UP_PIECES * X_SIZE
-    up_end = up_every + 2 * UP_PIECES * (16 - X_SIZE)
+    up_end = up_every + 3 * UP_PIECES * (16 - X_SIZE)
 
     def w_step(n):
         step, piece = lax.div(n, DOWN_PIECES) + 1, lax.rem(n, DOWN_PIECES)
@@ -304,9 +304,9 @@
             group = lax.div(n - w_first_steps, DOWN_PIECES)
             down_in.main_step(lax.div(group, Z_SIZE) + 1, lax.rem(group, Z_SIZE), piece)
 
-        @pl.when((n >= up_start) & ((n < up_every) | ((lax.rem(n, 2) == 0) & (n < up_end))))
-        def _():
-            m = jnp.where(n < up_every, n - up_start, UP_PIECES * X_SIZE + lax.div(n - up_every, 2))
+        @pl.when((n >= up_start) & ((n < up_every) | ((lax.rem(n - up_every, 3) == 0) & (n < up_end))))
+        def _():
+            m = jnp.where(n < up_every, n - up_start, UP_PIECES * X_SIZE + lax.div(n - up_every, 3))
             group = lax.div(m, UP_PIECES)
             up_in.main_step(
                 lax.div(group, X_SIZE) + 1, lax.rem(group, X_SIZE), lax.rem(m, UP_PIECES)
@@ -408,7 +408,7 @@
             ),
         )
 
-    busy = w_first_steps - DOWN_PIECES
+    busy = 14
 
     def for_others(n, _):
         w_loop(
@@ -444,7 +444,7 @@
         return 0
 
     def for_own(n, _):
-        w_loop(w_others + 4 * n, w_others + 4 * n + 4)
+        w_loop(w_others + 2 * n, w_others + 2 * n + 2)
         newer = here - 1 - 2 * n
 
         @pl.when(newer >= 1)
@@ -457,7 +457,7 @@
 
         return 0
 
-    w_others = w_first_steps
+    w_others = DOWN_PIECES + busy
     lax.fori_loop(0, 24, for_others, 0)
     acc[...] = jnp.zeros_like(acc)
     carry[...] = jnp.zeros_like(carry)
@@ -490,7 +490,7 @@
         remote(
             attg.at[tp], attg.at[tp], att_send.at[d - 1], att_recv.at[d - 1], peers[d - 1]
         ).start()
-    w_loop(w_others + 32, w_steps - 14)
+    w_loop(w_others + 16, 80)
     waits(owg.at[0:3, 0], ow_pair_recv)
     for d in (1, 2, 3):
         block = resg.at[tp]
@@ -513,12 +513,16 @@
     for b in range(4):
         mi[:, b * 512 : b * 512 + 512] = (hid[b].astype(F32) * inverse * mg_ref[b]).astype(BF16)
 
-    w_loop(w_steps - 14, w_steps)
-    waits(wg.at[0:4], pair_recv.at[0])
-    for b in range(4):
-        lifted = jnp.dot(mi[...], wg[(5, 6, 7, 4)[b]], preferred_element_type=F32)
+    def up(b):
+        lifted = jnp.dot(mi[...], wg[(6, 7, 4, 5)[b]], preferred_element_type=F32)
         lifted = jnp.maximum(lifted, 0.0)
         act[b] = (lifted * lifted).astype(BF16)
+
+    w_loop(80, w_steps)
+    waits(wg.at[0:2, 0:1024, :], pair_recv.at[1])
+    waits(wg.at[0:6, 0:1024, :], pair_recv.at[0])
+    for b in range(4):
+        up(b)
 
     def down(owner):
         rows = pl.ds(pl.multiple_of(owner * 512, 512), 512)
@@ -577,8 +581,9 @@
     for gather in (up_in, down_in):
         for phase in range(2):
             for d in range(2):
-                waits(wg.at[0, 0 : 32 * gather.sent(phase, d), :], gather.sem(phase, d))
-    waits(wg.at[0:4], pair_send.at[0])
+                waits(wg.at[0:2, 0 : 16 * gather.sent(phase, d), :], gather.sem(phase, d))
+    waits(wg.at[0:6, 0:1024, :], pair_send.at[0])
+    waits(wg.at[0:2, 0:1024, :], pair_send.at[1])
     waits(kvg.at[0], kv_send.at[2])
     for d in range(2):
         waits(kvg.at[0:3], kv_send.at[d])
@@ -596,7 +601,7 @@
 
     waits(owg.at[0:3, 0], ow_pair_send)
     for d in (1, 2, 3):
-        waits(res_ref, res_send.at[d - 1])
+        waits(resg.at[0], res_send.at[d - 1])
         waits(owg.at[0, 0], ow_send.at[d - 1])
         waits(attg.at[0], att_send.at[d - 1])
 
@@ -610,7 +615,9 @@
     return pl.pallas_call(
         kernel,
         out_shape=jax.ShapeDtypeStruct((256, 512), BF16),
-        in_specs=[pl.BlockSpec(memory_space=vmem)] * 10,
+        in_specs=[
+            pl.BlockSpec(memory_space=pl.ANY if n in (0, 6) else vmem) for n in range(10)
+        ],
         out_specs=pl.BlockSpec(memory_space=vmem),
         scratch_shapes=[
             vmem((KV_ROWS, 128), BF16),
@@ -650,8 +657,8 @@
             dma((2, 4, DOWN_PIECES)),
             dma((2, 2, Z_SIZE, DOWN_PIECES)),
             dma((8,)),
-            dma((1,)),
-            dma((1,)),
+            dma((2,)),
+            dma((2,)),
             dma((14,)),
             dma((3,)),
             dma((3,)),

time: 99.5 us -> 98.2 us (0.987)
  the two profiles are of different devices: /device:TPU:97 before, /device:TPU:1 now
where the time goes in v5:
time: 98.2 us; the launch traced here: 97.8 us
  Pallas kernels  96.1 us (98%)
  local copies, waits for them, and re-layouts  1.67 us (2%)
    pallas_call x1, Pallas kernels, body(): pl.pallas_call(kernel, out_shape=jax.ShapeDtypeStruct((256, 512), BF16),...  96.1 us

profile of v5, /device:TPU:1, one launch (start us, length us, event | category | flops | bytes accessed | tf_op | source)
XLA Modules:
  0.0 97.8 jit_solution(7056431772642759004)
XLA Ops:
  0.0 96.1 %layer.1 = bf16[256,512]{1,0:T(8,128)(2,1)} custom-call(bf16[256,512]{1,0:T(8,128)(2,1)} %res_ref.1, bf16[256,256]{1,0:T(8,128)(2,1)} %q_ref.1, bf16[256,128]{1,0:T(8,128)(2,1)} %k_ref.1, bf16[256,128]{1,0:T(8,128)(2,1)} %v_ref.1, bf16[1,256]{1,0:T(2,128)(2,1)} %shift_ref.1, f32[1,256]{1,0:T(1,128)} %bitcast.5, bf16[256,2048]{1,0:T(8,128)(2,1)} %ow_ref.1, ...), custom_call_target="tpu_custom_call" | custom-call | tf_op jit(solution)/shard_map/layer/pallas_call | solution.py:615
  96.2 1.7 %copy.12 = bf16[256,512]{1,0:T(8,128)(2,1)} copy(bf16[256,512]{1,0:T(8,128)(2,1)} %layer.1) | data formatting | bytes 524288

commit v6 on v5

--- a/solution.py
+++ b/solution.py
@@ -335,8 +335,8 @@
     up_in.own_near()
     down_in.own_near()
     lax.fori_loop(0, KV_PIECES, far_sides, 0)
+    down_in.own_main()
     up_in.own_first()
-    down_in.own_main()
     w_loop(0, DOWN_PIECES)
     lax.fori_loop(0, KV_PIECES, last_side, 0)
     half = pl.ds(pl.multiple_of(core * 1024, 1024), 1024)
@@ -408,7 +408,7 @@
             ),
         )
 
-    busy = 14
+    busy = 16
 
     def for_others(n, _):
         w_loop(

time: 98.2 us -> 98.4 us (level)
  no operation moved by 1% of the time
where the time goes in v6:
time: 98.4 us; the launch traced here: 98.3 us
  Pallas kernels  96.6 us (98%)
  local copies, waits for them, and re-layouts  1.67 us (2%)
    pallas_call x1, Pallas kernels, body(): pl.pallas_call(kernel, out_shape=jax.ShapeDtypeStruct((256, 512), BF16),...  96.6 us

profile of v6, /device:TPU:1, one launch (start us, length us, event | category | flops | bytes accessed | tf_op | source)
XLA Modules:
  0.0 98.3 jit_solution(8505256626006180283)
XLA Ops:
  0.0 96.6 %layer.1 = bf16[256,512]{1,0:T(8,128)(2,1)} custom-call(bf16[256,512]{1,0:T(8,128)(2,1)} %res_ref.1, bf16[256,256]{1,0:T(8,128)(2,1)} %q_ref.1, bf16[256,128]{1,0:T(8,128)(2,1)} %k_ref.1, bf16[256,128]{1,0:T(8,128)(2,1)} %v_ref.1, bf16[1,256]{1,0:T(2,128)(2,1)} %shift_ref.1, f32[1,256]{1,0:T(1,128)} %bitcast.5, bf16[256,2048]{1,0:T(8,128)(2,1)} %ow_ref.1, ...), custom_call_target="tpu_custom_call" | custom-call | tf_op jit(solution)/shard_map/layer/pallas_call | solution.py:615
  96.6 1.7 %copy.12 = bf16[256,512]{1,0:T(8,128)(2,1)} copy(bf16[256,512]{1,0:T(8,128)(2,1)} %layer.1) | data formatting | bytes 524288
